TPU v7x, 512 devices: a 8x2x16 block of a 8x16x16 slice. The times are simulated.
512 devices in a mesh: grp: 2 (over y), ep: 16 (over z), tp: 16 (over x, core).
Axes of the slice: x: 8, y: 2, z: 16, core: 2. Of those that a mesh axis runs over, the one named last changes fastest.
The devices are a block of a 8x16x16 slice.
Arguments:
- tokens: bfloat16 [192, 2048], P('grp', 'ep'), parts along dimension 0, may hold values from -70 to 70
- first_gain: float32 [2048], replicated, may hold values from 0.1 to 1.9
- w_query: bfloat16 [2048, 2048], P('ep', 'tp'), may hold values from -0.125 to 0.125
- w_key: bfloat16 [2048, 2048], P('ep', 'tp'), may hold values from -0.125 to 0.125
- w_value: bfloat16 [2048, 4096], P('ep', 'tp'), may hold values from -0.125 to 0.125
- w_outgate: bfloat16 [2048, 4096], P('ep', 'tp'), may hold values from -0.125 to 0.125
- w_input: bfloat16 [2048, 16], replicated, may hold values from -0.125 to 0.125
- w_forget: bfloat16 [2048, 16], replicated, may hold values from -0.125 to 0.125
- input_bias: float32 [16], replicated, may hold values from -3 to 3
- forget_bias: float32 [16], replicated, may hold values from -2 to 5
- head_gain: float32 [4096], replicated, may hold values from 0.1 to 1.9
- w_project: bfloat16 [4096, 2048], P('tp', 'ep'), may hold values from -0.09375 to 0.09375
- cell_state: float32 [192, 16, 128, 256], P(('grp', 'ep'), 'tp'), parts along dimension 0, may hold values from -6 to 6
- norm_state: float32 [192, 16, 128], P(('grp', 'ep'), 'tp'), parts along dimension 0, may hold values from -6 to 6
- max_state: float32 [192, 16], P(('grp', 'ep'), 'tp'), parts along dimension 0, may hold values from -110 to 110
- second_gain: float32 [2048], replicated, may hold values from 0.1 to 1.9
- routes: int32 [192, 2], P('grp'), parts along dimension 0, may hold values from 0 to 15, all different within a row; in each aligned block of 6 rows (0 to 5, 6 to 11, ...) at most 2 rows name the same one
- route_weight: float32 [192, 2], P('grp'), parts along dimension 0, may hold values from 0.2 to 1
- expert_gate: bfloat16 [16, 2048, 4096], P('ep', None, 'tp'), may hold values from -0.125 to 0.125
- expert_up: bfloat16 [16, 2048, 4096], P('ep', None, 'tp'), may hold values from -0.125 to 0.125
- expert_down: bfloat16 [16, 4096, 2048], P('ep', 'tp'), may hold values from -0.09375 to 0.09375
Outputs:
- layer_out: bfloat16 [192, 2048], P('grp', 'ep'), parts along dimension 0
- new_cell: float32 [192, 16, 128, 256], P(('grp', 'ep'), 'tp'), parts along dimension 0
- new_norm: float32 [192, 16, 128], P(('grp', 'ep'), 'tp'), parts along dimension 0
- new_max: float32 [192, 16], P(('grp', 'ep'), 'tp'), parts along dimension 0
There are 2 independent parts, one for each index of `grp`. A program takes and returns all parts, laid end to end along the dimension named above; an argument that names none is the same for every part. Nothing has to cross between parts.
Inputs may be any that keep to these rules, and one draw needn't show every extreme that they name: `routes`: each sequence names 2 different experts. In each aligned block of 6 sequences no expert is named by more than 2 of them, a bound that some block reaches.
All inputs are finite; a program needn't handle non-finite values.
Results may differ from a plain program's by a relative error of at most 0.0065.
Values may be sent and summed in bfloat16 or wider, within the bound.
A program may use at most 64 MiB of HBM per device.

v0:
```python
import jax
import jax.numpy as jnp
from jax import lax
from jax.sharding import PartitionSpec as P

EXP_DEV = 1


NORM_EPS = 1e-05
HEAD_EPS = 1e-06


def from_everyone(array, axis):
    peers = lax.axis_size(axis)
    return lax.all_to_all(
        jnp.broadcast_to(array[None], (peers, *array.shape)), axis, 0, 0, tiled=True
    )


def taken_together(array, axis):
    everything = from_everyone(array, axis)
    return jnp.sum(everything, axis=0)


def in_one(arrays, axis):
    ends = [0]
    for a in arrays:
        ends.append(ends[-1] + a.size)
    subtotal = taken_together(jnp.concatenate([a.ravel() for a in arrays]), axis)
    return tuple((subtotal[b:e].reshape(a.shape) for a, b, e in zip(arrays, ends, ends[1:])))


def cut_along(array, dim, peers):
    lengths = array.shape
    blocks = array.reshape(*lengths[:dim], peers, lengths[dim] // peers, *lengths[dim + 1 :])
    return jnp.moveaxis(blocks, dim, 0)


def summed_on_arrival(array, axis, dim):
    blocks = cut_along(array, dim, lax.axis_size(axis))
    arrived = lax.all_to_all(blocks, axis, split_axis=0, concat_axis=0, tiled=True)
    return arrived.astype(jnp.float32).sum(axis=0)


def summed_on_arrival_2(array, axis, dim):
    blocks = cut_along(array, dim, lax.axis_size(axis))
    arrived = lax.all_to_all(blocks, axis, split_axis=0, concat_axis=0, tiled=True)
    return arrived.sum(axis=0)


def side_by_side(arrays, axis, dim, along):
    ends, at = ([], 0)
    for a in arrays[:-1]:
        at += a.shape[along]
        ends.append(at)
    both = jnp.concatenate(arrays, axis=along)
    return tuple(jnp.split(summed_on_arrival_2(both, axis, dim), ends, axis=along))


def joined_along(blocks, dim):
    lengths = list(blocks.shape[1:])
    lengths[dim] *= blocks.shape[0]
    return jnp.moveaxis(blocks, 0, dim).reshape(lengths)


def gather_directly(array, axis, dim):
    return joined_along(from_everyone(array, axis), dim)


def gathered_total(array, axis):
    blocks = lax.all_gather(array, axis)
    return blocks.sum(axis=0)


def row_norm(stream_rows, gain_whole):
    col_count = stream_rows.shape[1]
    gain_cols = lax.dynamic_slice_in_dim(gain_whole, lax.axis_index("ep") * col_count, col_count, 0)
    values = stream_rows.astype(jnp.float32)
    totals, squares = in_one((jnp.sum(values, axis=1), jnp.sum(values * values, axis=1)), "ep")
    features = col_count * lax.axis_size("ep")
    row_mean = totals / features
    spread = squares / features - row_mean * row_mean
    inv_scale = lax.rsqrt(spread + NORM_EPS)
    return ((values - row_mean[:, None]) * inv_scale[:, None] * gain_cols).astype(jnp.bfloat16)


def expert_act(gate_sum, up_sum):
    return (jax.nn.silu(gate_sum) * up_sum).astype(jnp.bfloat16)


def scatter_slots(active, expert_down):
    slot_major = jnp.moveaxis(active, 1, 0)
    return summed_on_arrival(
        jnp.einsum(
            "pef,efd->ped", slot_major, expert_down, preferred_element_type=jnp.float32
        ).astype(jnp.bfloat16),
        "tp",
        0,
    ).astype(jnp.bfloat16)


def on_device(
    tokens,
    first_gain,
    w_query,
    w_key,
    w_value,
    w_outgate,
    w_input,
    w_forget,
    input_bias,
    forget_bias,
    head_gain,
    w_project,
    cell_state,
    norm_state,
    max_state,
    second_gain,
    routes,
    route_weight,
    expert_gate,
    expert_up,
    expert_down,
):
    blocks = lax.axis_size("ep")
    columns = tokens.shape[1]
    seq_total = tokens.shape[0]
    seq_local = seq_total // blocks
    heads_local = cell_state.shape[1]
    key_size = cell_state.shape[2]
    value_size = cell_state.shape[3]
    col_start = lax.axis_index("ep") * columns
    head_start = lax.axis_index("tp") * heads_local
    normed = row_norm(tokens, first_gain)
    input_cols = lax.dynamic_slice(w_input, (col_start, head_start), (columns, heads_local))
    forget_cols = lax.dynamic_slice(w_forget, (col_start, head_start), (columns, heads_local))

    def project_part(weight):
        return jnp.dot(normed, weight, preferred_element_type=jnp.float32)

    summed = side_by_side(
        (
            project_part(w_query),
            project_part(w_key),
            project_part(w_value),
            project_part(w_outgate),
            project_part(input_cols),
            project_part(forget_cols),
        ),
        "ep",
        0,
        1,
    )
    queries = summed[0].astype(jnp.bfloat16).reshape(seq_local, heads_local, key_size)
    key_rows = summed[1].astype(jnp.bfloat16).reshape(seq_local, heads_local, key_size)
    value_rows = summed[2].astype(jnp.bfloat16).reshape(seq_local, heads_local, value_size)
    outgate = summed[3].astype(jnp.bfloat16)
    input_pre = summed[4] + lax.dynamic_slice_in_dim(input_bias, head_start, heads_local, 0)
    forget_pre = summed[5] + lax.dynamic_slice_in_dim(forget_bias, head_start, heads_local, 0)
    carried = jax.nn.log_sigmoid(forget_pre) + max_state
    new_max = jnp.maximum(carried, input_pre)
    keep_old = jnp.exp(carried - new_max)
    admit_new = jnp.exp(input_pre - new_max)
    key_float = key_rows.astype(jnp.float32)
    value_float = value_rows.astype(jnp.float32)
    new_cell = (
        keep_old[:, :, None, None] * cell_state
        + admit_new[:, :, None, None] * key_float[:, :, :, None] * value_float[:, :, None, :]
    )
    new_norm = keep_old[:, :, None] * norm_state + admit_new[:, :, None] * key_float
    query_float = queries.astype(jnp.float32) * key_size ** (-0.5)
    readout = jnp.einsum("shk,shkv->shv", query_float, new_cell, precision=lax.Precision.HIGHEST)
    head_mean = jnp.mean(readout, axis=2, keepdims=True)
    centred = readout - head_mean
    head_var = jnp.mean(centred * centred, axis=2, keepdims=True)
    gains_here = lax.dynamic_slice_in_dim(
        head_gain, head_start * value_size, heads_local * value_size, 0
    )
    mixed_heads = (
        (centred * lax.rsqrt(head_var + HEAD_EPS)).reshape(seq_local, heads_local * value_size)
        * gains_here
        * jax.nn.sigmoid(outgate.astype(jnp.float32))
    ).astype(jnp.bfloat16)
    head_terms = jnp.dot(
        gather_directly(mixed_heads, "ep", 0), w_project, preferred_element_type=jnp.float32
    )
    mixer_out = gathered_total(head_terms, "tp")
    stream = (tokens.astype(jnp.float32) + mixer_out).astype(jnp.bfloat16)
    second_normed = row_norm(stream, second_gain)
    experts = blocks * EXP_DEV
    top_count = routes.shape[1]
    capacity = max(2, 2 * seq_local * top_count // experts)
    slot_count = blocks * capacity
    expert_ids = lax.broadcasted_iota(jnp.int32, (1, 1, experts), 2)
    matches = routes[:, :, None] == expert_ids
    routed = jnp.sum(matches.astype(jnp.int32), axis=1)
    combine = jnp.sum(jnp.where(matches, route_weight[:, :, None], 0.0), axis=1)
    running = (
        jnp.cumsum(routed.reshape(blocks, seq_local, experts), axis=1).reshape(seq_total, experts)
        - routed
    )
    block_ids = lax.broadcasted_iota(jnp.int32, (seq_total, experts), 0) // seq_local
    slot_of = block_ids * capacity + running
    slot_ids = lax.broadcasted_iota(jnp.int32, (experts, slot_count, seq_total), 1)
    placed = (slot_of.T[:, None, :] == slot_ids) & (routed.T[:, None, :] > 0)
    picker = placed.astype(jnp.bfloat16)
    weighted = jnp.where(placed, combine.T[:, None, :], 0.0)
    outbound = jnp.einsum(
        "eps,sd->epd", picker, second_normed, preferred_element_type=jnp.float32
    ).astype(jnp.bfloat16)
    arrived = lax.all_to_all(outbound, "ep", split_axis=0, concat_axis=2, tiled=True)
    gate_sum = jnp.einsum("end,edf->enf", arrived, expert_gate, preferred_element_type=jnp.float32)
    up_sum = jnp.einsum("end,edf->enf", arrived, expert_up, preferred_element_type=jnp.float32)
    active = expert_act(gate_sum, up_sum)
    share = scatter_slots(active, expert_down)
    back = lax.all_to_all(share, "ep", split_axis=2, concat_axis=1, tiled=True)
    every_slot = gather_directly(back, "tp", 0)
    moe_out = jnp.einsum(
        "eps,ped->sd", weighted, every_slot.astype(jnp.float32), precision=lax.Precision.HIGHEST
    )
    layer_out = (stream.astype(jnp.float32) + moe_out).astype(jnp.bfloat16)
    return (layer_out, new_cell, new_norm, new_max)


def solution(mesh):
    placed = (
        P("grp", "ep"),
        P(),
        P("ep", "tp"),
        P("ep", "tp"),
        P("ep", "tp"),
        P("ep", "tp"),
        P(),
        P(),
        P(),
        P(),
        P(),
        P("tp", "ep"),
        P(("grp", "ep"), "tp", None, None),
        P(("grp", "ep"), "tp", None),
        P(("grp", "ep"), "tp"),
        P(),
        P("grp", None),
        P("grp", None),
        P("ep", None, "tp"),
        P("ep", None, "tp"),
        P("ep", "tp", None),
    )
    return jax.shard_map(
        on_device,
        mesh=mesh,
        in_specs=placed,
        out_specs=(
            P("grp", "ep"),
            P(("grp", "ep"), "tp", None, None),
            P(("grp", "ep"), "tp", None),
            P(("grp", "ep"), "tp"),
        ),
        check_vma=False,
    )
```

profile of v0, /device:TPU:65, one launch (start us, length us, event | category | flops | bytes accessed | tf_op | source)
XLA Modules:
  0.0 232.7 jit_solution(2197950431508416456)
XLA Ops:
  0.6 0.9 convert_reduce_fusion.1
  1.7 0.6 broadcast_in_dim.26
  2.3 44.2 %all-to-all-start = ((f32[16,1,192]{2,1,0:T(1,128)}), f32[16,1,192]{2,1,0:T(1,128)S(1)}, u32[]{:S(2)}, u32[]{:S(2)}) async-start(f32[16,1,192]{2,1,0:T(1,128)} %broadcast_in_dim.26), calls=%async_computation | async-start | bytes 32768 | tf_op jit(solution)/shard_map/all_to_all | solution.py:15
  46.5 0.8 dynamic_slice.21
  47.3 10.4 %all-to-all-done = f32[16,1,192]{2,1,0:T(1,128)S(1)} async-done(((f32[16,1,192]{2,1,0:T(1,128)}), f32[16,1,192]{2,1,0:T(1,128)S(1)}, u32[]{:S(2)}, u32[]{:S(2)}) %all-to-all-start) | async-done | bytes 12320 | tf_op jit(solution)/shard_map/all_to_all | solution.py:15
  57.8 0.1 fusion.30
  57.9 0.9 fusion.46
  58.8 0.1 copy.110
  58.9 0.9 fusion.48
  59.8 0.1 copy.109
  59.9 0.6 copy-done.9
  60.6 0.1 fusion.71
  60.7 0.7 copy-done.10
  61.5 0.1 fusion.70
  61.6 0.1 copy.93
  61.8 0.1 copy.94
  61.9 0.6 copy-done.6
  62.5 0.1 fusion.73
  62.6 0.8 copy-done.7
  63.5 0.1 fusion.72
  63.6 0.9 concatenate.23
  64.5 4.1 %all-to-all-start.1 = ((f32[16,6,770]{2,1,0:T(8,128)}), f32[16,6,770]{2,1,0:T(8,128)S(1)}, u32[]{:S(2)}, u32[]{:S(2)}) async-start(f32[16,6,770]{2,1,0:T(8,128)} %concatenate.23), calls=%async_computation.1 | async-start | bytes 917504 | tf_op jit(solution)/shard_map/all_to_all | solution.py:47
  68.6 0.6 copy-done.15
  69.3 0.6 dynamic_slice.24
  69.9 0.6 dynamic_slice.25
  70.7 0.6 copy-done.11
  71.3 0.1 copy.96
  71.5 0.8 dynamic_slice.26
  72.3 17.0 %all-to-all-done.1 = f32[16,6,770]{2,1,0:T(8,128)S(1)} async-done(((f32[16,6,770]{2,1,0:T(8,128)}), f32[16,6,770]{2,1,0:T(8,128)S(1)}, u32[]{:S(2)}, u32[]{:S(2)}) %all-to-all-start.1) | async-done | bytes 295712 | tf_op jit(solution)/shard_map/all_to_all | solution.py:47
  89.3 1.5 exponential_reduce_fusion.1
  90.9 0.2 multiply_add_fusion
  91.1 0.5 fusion.9
  91.6 0.1 bitcast_reduce_fusion
  91.8 0.2 fusion.53
  92.0 0.6 broadcast_in_dim.27
  92.7 11.5 %all-to-all-start.2 = ((bf16[16,6,256]{2,1,0:T(8,128)(2,1)}), bf16[16,6,256]{2,1,0:T(8,128)(2,1)S(1)}, u32[]{:S(2)}, u32[]{:S(2)}) async-start(bf16[16,6,256]{2,1,0:T(8,128)(2,1)} %broadcast_in_dim.27), calls=%async_computation.2 | async-start | bytes 131072 | tf_op jit(solution)/shard_map/all_to_all | solution.py:15
  104.2 11.4 %all-to-all-done.2 = bf16[16,6,256]{2,1,0:T(8,128)(2,1)S(1)} async-done(((bf16[16,6,256]{2,1,0:T(8,128)(2,1)}), bf16[16,6,256]{2,1,0:T(8,128)(2,1)S(1)}, u32[]{:S(2)}, u32[]{:S(2)}) %all-to-all-start.2) | async-done | bytes 49184 | tf_op jit(solution)/shard_map/all_to_all | solution.py:15
  115.6 0.1 fusion.74
  115.7 22.3 %all-gather = f32[1536,128]{1,0:T(8,128)S(1)} all-gather(f32[96,128]{1,0:T(8,128)S(1)} %fusion.74), channel_id=2, replica_groups=mesh['grp'=2,'ep'=16,'tp'=16] {'tp'}, dimensions={0}, use_global_device_ids=true | all-gather | bytes 835584 | tf_op jit(solution)/shard_map/all_gather | solution.py:71
  138.1 0.1 convert_reduce_fusion
  138.3 0.6 broadcast_in_dim.32
  139.0 3.9 %all-to-all-start.3 = ((f32[16,1,192]{2,1,0:T(1,128)}), f32[16,1,192]{2,1,0:T(1,128)S(1)}, u32[]{:S(2)}, u32[]{:S(2)}) async-start(f32[16,1,192]{2,1,0:T(1,128)} %broadcast_in_dim.32), calls=%async_computation.3 | async-start | bytes 32768 | tf_op jit(solution)/shard_map/all_to_all | solution.py:15
  142.9 0.8 dynamic_slice.27
  143.7 10.2 %all-to-all-done.3 = f32[16,1,192]{2,1,0:T(1,128)S(1)} async-done(((f32[16,1,192]{2,1,0:T(1,128)}), f32[16,1,192]{2,1,0:T(1,128)S(1)}, u32[]{:S(2)}, u32[]{:S(2)}) %all-to-all-start.3) | async-done | bytes 12320 | tf_op jit(solution)/shard_map/all_to_all | solution.py:15
  154.0 0.3 convolution_convert_fusion.1
  154.3 14.6 %all_to_all.56 = bf16[16,32,128]{2,1,0:T(8,128)(2,1)S(1)} all-to-all(bf16[16,32,128]{2,1,0:T(8,128)(2,1)S(1)} %convolution_convert_fusion.1), channel_id=1, replica_groups=mesh['grp'=2,'ep'=16,'tp'=16] {'ep'}, dimensions={0} | all-to-all | bytes 262144 | tf_op jit(solution)/shard_map/all_to_all | solution.py:211
  168.9 0.3 fusion.7
  169.2 0.7 fusion
  169.9 0.1 reshape.205
  170.1 16.3 %all_to_all.57 = bf16[16,2,1,2048]{3,1,2,0:T(2,128)(2,1)S(1)} all-to-all(bf16[16,2,1,2048]{3,1,2,0:T(2,128)(2,1)S(1)} %bitcast.105), channel_id=1, replica_groups=mesh['grp'=2,'ep'=16,'tp'=16] {'tp'}, dimensions={0} | all-to-all | bytes 262144 | tf_op jit(solution)/shard_map/all_to_all | solution.py:41
  186.4 0.1 reduce_sum.134
  186.5 0.9 copy.101
  187.4 0.5 broadcast.140
  187.9 11.5 %reduce.12 = bf16[2048,2]{1,0:T(8,128)(2,1)S(1)} reduce(bf16[2048,1,2]{2,1,0:T(2,128)(2,1)S(1)} %bitcast.99, bf16[]{:T(256)} %broadcast.140), dimensions={1}, to_apply=%bitcast.86.reduce_sub_computation | reduce | bytes 16386
  199.4 0.6 reshape.218
  200.1 15.1 %all_to_all.58 = bf16[16,2,128]{2,1,0:T(2,128)(2,1)S(1)} all-to-all(bf16[16,2,128]{2,1,0:T(2,128)(2,1)S(1)} %reshape.218), channel_id=1, replica_groups=mesh['grp'=2,'ep'=16,'tp'=16] {'ep'}, dimensions={0} | all-to-all | bytes 16384 | tf_op jit(solution)/shard_map/all_to_all | solution.py:216
  215.1 1.2 reshape.219
  216.4 0.6 copy.102
  217.0 0.7 broadcast_in_dim.34
  217.7 4.7 %all-to-all-start.7 = ((bf16[16,2,16,128]{3,1,2,0:T(2,128)(2,1)}), bf16[16,2,16,128]{3,1,2,0:T(2,128)(2,1)S(1)}, u32[]{:S(2)}, u32[]{:S(2)}) async-start(bf16[16,2,16,128]{3,1,2,0:T(2,128)(2,1)} %broadcast_in_dim.34), calls=%async_computation.7 | async-start | bytes 262144 | tf_op jit(solution)/shard_map/all_to_all | solution.py:15
  222.4 0.6 copy.107
  223.2 0.6 copy.106
  223.7 7.9 %all-to-all-done.7 = bf16[16,2,16,128]{3,1,2,0:T(2,128)(2,1)S(1)} async-done(((bf16[16,2,16,128]{3,1,2,0:T(2,128)(2,1)}), bf16[16,2,16,128]{3,1,2,0:T(2,128)(2,1)S(1)}, u32[]{:S(2)}, u32[]{:S(2)}) %all-to-all-start.7) | async-done | bytes 131104 | tf_op jit(solution)/shard_map/all_to_all | solution.py:15
  231.7 1.0 fusion.2
  (62 shorter events, 1.5 us)
Async XLA Ops:
  0.6 168.6 %copy-start = (bf16[1,256,2048]{2,1,0:T(8,128)(2,1)S(1)}, bf16[1,256,2048]{2,1,0:T(8,128)(2,1)}, u32[]{:S(2)}) copy-start(bf16[1,256,2048]{2,1,0:T(8,128)(2,1)} %param.41) | copy-start | bytes 3145732
  2.3 55.4 %all-to-all-start = ((f32[16,1,192]{2,1,0:T(1,128)}), f32[16,1,192]{2,1,0:T(1,128)S(1)}, u32[]{:S(2)}, u32[]{:S(2)}) async-start(f32[16,1,192]{2,1,0:T(1,128)} %broadcast_in_dim.26), calls=%async_computation | async-start | bytes 32768 | tf_op jit(solution)/shard_map/all_to_all | solution.py:15
  46.5 11.3 %copy-start.5 = (bf16[96,128]{1,0:T(8,128)(2,1)S(1)}, bf16[96,128]{1,0:T(8,128)(2,1)}, u32[]{:S(2)}) copy-start(bf16[96,128]{1,0:T(8,128)(2,1)} %param.21) | copy-start | bytes 73732
  59.8 0.8 copy-start.9
  60.7 0.8 copy-start.10
  61.6 0.8 copy-start.6
  62.6 0.9 copy-start.7
  64.5 26.5 %copy-start.4 = (f32[6,1,128,256]{3,2,1,0:T(8,128)S(1)}, f32[6,1,128,256]{3,2,1,0:T(8,128)}, u32[]{:S(2)}) copy-start(f32[6,1,128,256]{3,2,1,0:T(8,128)} %param.33) | copy-start | bytes 2359300
  64.5 24.8 %all-to-all-start.1 = ((f32[16,6,770]{2,1,0:T(8,128)}), f32[16,6,770]{2,1,0:T(8,128)S(1)}, u32[]{:S(2)}, u32[]{:S(2)}) async-start(f32[16,6,770]{2,1,0:T(8,128)} %concatenate.23), calls=%async_computation.1 | async-start | bytes 917504 | tf_op jit(solution)/shard_map/all_to_all | solution.py:47
  68.6 0.7 copy-start.15
  69.3 0.7 copy-start.16
  69.9 0.7 copy-start.14
  70.6 0.7 copy-start.11
  91.1 46.9 %copy-start.1 = (f32[6,1,128,256]{3,2,1,0:T(8,128)}, f32[6,1,128,256]{3,2,1,0:T(8,128)S(1)}, u32[]{:S(2)}) copy-start(f32[6,1,128,256]{3,2,1,0:T(8,128)S(1)} %multiply_add_fusion) | copy-start | bytes 2359300
  92.7 22.9 %all-to-all-start.2 = ((bf16[16,6,256]{2,1,0:T(8,128)(2,1)}), bf16[16,6,256]{2,1,0:T(8,128)(2,1)S(1)}, u32[]{:S(2)}, u32[]{:S(2)}) async-start(bf16[16,6,256]{2,1,0:T(8,128)(2,1)} %broadcast_in_dim.27), calls=%async_computation.2 | async-start | bytes 131072 | tf_op jit(solution)/shard_map/all_to_all | solution.py:15
  104.2 11.4 %copy-start.8 = (bf16[256,128]{1,0:T(8,128)(2,1)S(1)}, bf16[256,128]{1,0:T(8,128)(2,1)}, u32[]{:S(2)}) copy-start(bf16[256,128]{1,0:T(8,128)(2,1)} %param.32) | copy-start | bytes 196612
  138.1 30.8 %copy-start.3 = (bf16[1,2048,256]{2,1,0:T(8,128)(2,1)S(1)}, bf16[1,2048,256]{2,1,0:T(8,128)(2,1)}, u32[]{:S(2)}) copy-start(bf16[1,2048,256]{2,1,0:T(8,128)(2,1)} %param.39) | copy-start | bytes 3145732
  138.2 31.0 %copy-start.2 = (bf16[1,2048,256]{2,1,0:T(8,128)(2,1)S(1)}, bf16[1,2048,256]{2,1,0:T(8,128)(2,1)}, u32[]{:S(2)}) copy-start(bf16[1,2048,256]{2,1,0:T(8,128)(2,1)} %param.40) | copy-start | bytes 3145732
  139.0 14.9 %all-to-all-start.3 = ((f32[16,1,192]{2,1,0:T(1,128)}), f32[16,1,192]{2,1,0:T(1,128)S(1)}, u32[]{:S(2)}, u32[]{:S(2)}) async-start(f32[16,1,192]{2,1,0:T(1,128)} %broadcast_in_dim.32), calls=%async_computation.3 | async-start | bytes 32768 | tf_op jit(solution)/shard_map/all_to_all | solution.py:15
  217.7 4.7 %copy-start.13 = (f32[96,2]{0,1:T(2,128)S(1)}, f32[96,2]{0,1:T(2,128)}, u32[]{:S(2)}) copy-start(f32[96,2]{0,1:T(2,128)} %param.38) | copy-start | bytes 2308
  217.7 13.9 %all-to-all-start.7 = ((bf16[16,2,16,128]{3,1,2,0:T(2,128)(2,1)}), bf16[16,2,16,128]{3,1,2,0:T(2,128)(2,1)S(1)}, u32[]{:S(2)}, u32[]{:S(2)}) async-start(bf16[16,2,16,128]{3,1,2,0:T(2,128)(2,1)} %broadcast_in_dim.34), calls=%async_computation.7 | async-start | bytes 262144 | tf_op jit(solution)/shard_map/all_to_all | solution.py:15
  222.4 0.7 copy-start.12
where the time goes:
time: 234 us; the launch traced here: 233 us
  starting transfers between devices  68.5 us (29%)
  blocking collectives  68.3 us (29%)
  waiting for transfers between devices  56.8 us (24%)
  local copies, waits for them, and re-layouts  17.4 us (7%)
  other arithmetic  15.6 us (7%)
  matrix products  5.14 us (2%)
    all_to_all x4, starting transfers between devices, from_everyone(): lax.all_to_all(jnp.broadcast_to(array[None], (peers, *array.shape)), axis...  64.3 us
    all_to_all x4, waiting for transfers between devices, from_everyone(): lax.all_to_all(jnp.broadcast_to(array[None], (peers, *array.shape)), axis...  39.9 us
    all_gather x1, blocking collectives, gathered_total(): blocks = lax.all_gather(array, axis)  22.3 us
    all_to_all x1, waiting for transfers between devices, summed_on_arrival_2(): lax.all_to_all(blocks, axis, split_axis=0, concat_axis=0, tiled=True)  17 us
    all_to_all x1, blocking collectives, summed_on_arrival(): lax.all_to_all(blocks, axis, split_axis=0, concat_axis=0, tiled=True)  16.3 us
    all_to_all x1, blocking collectives, on_device(): back = lax.all_to_all(share, 'ep', split_axis=2, concat_axis=1, tiled=True)  15.1 us
    all_to_all x1, blocking collectives, on_device(): lax.all_to_all(outbound, 'ep', split_axis=0, concat_axis=2, tiled=True)  14.6 us
    unnamed x1, other arithmetic  11.5 us
  transfers between devices with their start and end apart: 5, of which 5 were waited for; matrix products, arithmetic and copies ran while one was open for 2% of the time, Pallas kernels for 0%

commit v1 on v0

v1 whole, which is shorter than its diff:
```python
import functools

import jax
import jax.numpy as jnp
from jax import lax
from jax.experimental import pallas as pl
from jax.experimental.pallas import tpu as pltpu
from jax.sharding import PartitionSpec as P

NORM_EPS = 1e-05
HEAD_EPS = 1e-06
F32 = jnp.float32
BF16 = jnp.bfloat16
LANES = 128
SUB = 8


def iota(shape, dim):
    return lax.broadcasted_iota(jnp.int32, shape, dim)


def total(x):
    return jnp.sum(jnp.sum(x, axis=1, keepdims=True), axis=0, keepdims=True)


def far_first(n):
    order = [n // 2]
    for d in range(1, n // 2):
        order += [n // 2 + d, n // 2 - d]
    if n % 2 == 0:
        return [d for d in order if 0 < d < n]
    return list(range(1, n))


def kernel(
    n_ep, n_tp, seq_local, key_size, value_size,
    tokens_h, gain1_h, wq_h, wk_h, wv_h, wo_h, win_h, wfg_h, ib_h, fb_h, hg_h, wp_h,
    cell_h, norm_h, max_h, gain2_h, routes_h, rw_h, eg_h, eu_h, ed_h,
    out_ref, ncell_ref, nnorm_ref, nmax_ref,
    tokens_v, gain1_v, wq_v, wk_v, wv_v, wo_v, win_v, wfg_v, ib_v, fb_v, hg_v, wp_v,
    cell_v, norm_v, max_v, gain2_v, routes_v, rw_v, eg_v, eu_v, ed_v,
    msg0, rec0, msgv, recv, msg1, rec1, msg2, rec2, msg3, rec3, msg4, rec4, msg5, rec5, msg6, rec6, msg7, rec7, msg8, rec8,
    t8_s, part_s, sum_s, slot_s, wide_s,
    load_sem, send_sem, recv_sem,
):
    ep = lax.axis_index("ep")
    tp = lax.axis_index("tp")
    barrier = pltpu.get_barrier_semaphore()
    ep_peers = [lax.rem(ep + d, n_ep) for d in far_first(n_ep)]
    tp_peers = [lax.rem(tp + d, n_tp) for d in far_first(n_tp)]
    for peer in ep_peers:
        pl.semaphore_signal(barrier, inc=1, device_id={"ep": peer}, device_id_type=pl.DeviceIdType.MESH)
    for peer in tp_peers:
        pl.semaphore_signal(barrier, inc=1, device_id={"tp": peer}, device_id_type=pl.DeviceIdType.MESH)

    sources = (
        tokens_h, gain1_h, wq_h, wk_h, wv_h, wo_h, win_h, wfg_h, ib_h, fb_h, hg_h, wp_h,
        cell_h, norm_h, max_h, gain2_h, routes_h, rw_h, eg_h, eu_h, ed_h,
    )
    targets = (
        tokens_v, gain1_v, wq_v, wk_v, wv_v, wo_v, win_v, wfg_v, ib_v, fb_v, hg_v, wp_v,
        cell_v, norm_v, max_v, gain2_v, routes_v, rw_v, eg_v, eu_v, ed_v,
    )
    loads = [
        pltpu.make_async_copy(s, t, load_sem.at[i]) for i, (s, t) in enumerate(zip(sources, targets))
    ]
    for copy in loads:
        copy.start()

    def send(phase, axis, peers, source, target, each):
        me = ep if axis == "ep" else tp
        for peer in peers:
            pltpu.make_async_remote_copy(
                src_ref=source.at[peer] if each else source,
                dst_ref=target.at[me],
                send_sem=send_sem.at[phase],
                recv_sem=recv_sem.at[phase],
                device_id={axis: peer},
                device_id_type=pl.DeviceIdType.MESH,
            ).start()

    def arrive(phase, target):
        others = target.at[pl.ds(0, target.shape[0] - 1)]
        pltpu.make_async_copy(others, others, recv_sem.at[phase]).wait()

    def drain(phase, target):
        others = target.at[pl.ds(0, target.shape[0] - 1)]
        pltpu.make_async_copy(others, others, send_sem.at[phase]).wait()

    rows8 = max(SUB * n_ep, LANES)
    seqs = n_ep * seq_local
    features = n_ep * LANES
    nt = (((1,), (1,)), ((), ()))
    sub = iota((SUB, LANES), 0)
    lane = iota((SUB, LANES), 1)
    kt = key_size // LANES
    vt = value_size // LANES

    for copy in loads[:6]:
        copy.wait()
    r8 = iota((rows8, seqs), 0)
    pick = ((r8 // SUB) * seq_local + r8 % SUB == iota((rows8, seqs), 1)) & (r8 % SUB < seq_local)
    t8 = jnp.dot(pick.astype(BF16), tokens_v[...], preferred_element_type=F32)
    t8_s[...] = t8
    wide_lane = iota((rows8, LANES), 1)
    row_sum = jnp.sum(t8, axis=1, keepdims=True)
    row_square = jnp.sum(t8 * t8, axis=1, keepdims=True)
    stats = jnp.where(wide_lane == 0, row_sum, jnp.where(wide_lane == 1, row_square, 0.0)).T
    msg0[...] = stats[0:2]
    gain_here = gain1_v[pl.ds(ep, 1), :]
    gain_high = gain_here.astype(BF16).astype(F32)
    kind = iota((rows8, LANES), 0) % SUB
    centred = (t8 - row_sum * (1.0 / LANES)) * gain_here
    left = jnp.where(
        kind == seq_local, gain_high, jnp.where(kind == seq_local + 1, gain_here - gain_high, centred)
    ).astype(BF16)
    at = 0
    for w in (wv_v, wo_v):
        part = jnp.dot(left, w[...], preferred_element_type=F32)
        for j in range(vt):
            part_s[at] = part[:, j * LANES:(j + 1) * LANES]
            at += 1
    for j in range(2 * vt):
        gain_term = part_s[j, pl.ds(seq_local, 1), :] + part_s[j, pl.ds(seq_local + 1, 1), :]
        term_high = gain_term.astype(BF16).astype(F32)
        part_s[j, pl.ds(seq_local, n_ep, SUB), :] = jnp.broadcast_to(term_high, (n_ep, LANES))
        part_s[j, pl.ds(seq_local + 1, n_ep, SUB), :] = jnp.broadcast_to(
            gain_term - term_high, (n_ep, LANES)
        )
    for p in range(n_ep):
        rows = slice(p * SUB, (p + 1) * SUB)
        for j in range(vt):
            msgv[p, :, j * LANES:(j + 1) * LANES] = jnp.concatenate(
                [part_s[j, rows, :], part_s[vt + j, rows, :]], axis=0
            ).astype(BF16)

    pl.semaphore_wait(barrier, len(ep_peers) + len(tp_peers))
    send(0, "ep", ep_peers, msg0, rec0, False)
    send(9, "ep", ep_peers, msgv, recv, True)
    rec0[ep] = msg0[...]
    recv[ep] = msgv[ep]

    for copy in loads[6:18]:
        copy.wait()
    here = pl.ds(pl.multiple_of(ep * LANES, LANES), LANES)
    gate_w = jnp.zeros((SUB, LANES), F32)
    for row, source in enumerate((win_v, wfg_v)):
        head = (iota((SUB, n_tp), 1) == tp) & (iota((SUB, n_tp), 0) == row)
        gate_w = gate_w + jnp.dot(head.astype(BF16), source[:, here], preferred_element_type=F32)
    gate_w = gate_w.astype(BF16)
    at_head = iota((1, n_tp), 1) == tp
    input_bias = jnp.sum(jnp.where(at_head, ib_v[...], 0.0), axis=1, keepdims=True)
    forget_bias = jnp.sum(jnp.where(at_head, fb_v[...], 0.0), axis=1, keepdims=True)

    top = routes_v.shape[0]
    own_row = iota((SUB, seqs), 1) == tp * seq_local + iota((SUB, seqs), 0)
    own_row = own_row & (iota((SUB, seqs), 0) < seq_local)
    routed = jnp.zeros((SUB, LANES), F32)
    combine = jnp.zeros((SUB, LANES), F32)
    for k in range(top):
        named = jnp.sum(
            jnp.where(own_row, routes_v[k:k + 1, :].astype(F32) + 1.0, 0.0), axis=1, keepdims=True
        )
        weight = jnp.sum(jnp.where(own_row, rw_v[k:k + 1, :], 0.0), axis=1, keepdims=True)
        match = jnp.abs(named - 1.0 - (lane // SUB).astype(F32)) < 0.5
        routed = routed + jnp.where(match, 1.0, 0.0)
        combine = combine + jnp.where(match, weight, 0.0)
    before = (iota((SUB, SUB), 1) < iota((SUB, SUB), 0)).astype(BF16)
    running = jnp.dot(before, routed.astype(BF16), preferred_element_type=F32)
    placed = jnp.where((routed > 0.5) & (jnp.abs(running - (lane % SUB).astype(F32)) < 0.5), 1.0, 0.0)
    slot_weight = placed * combine
    weight_high = slot_weight.astype(BF16)
    rest = slot_weight - weight_high.astype(F32)
    weight_mid = rest.astype(BF16)
    weight_low = (rest - weight_mid.astype(F32)).astype(BF16)
    capacity = 2
    chosen = [
        jnp.sum(jnp.where(lane == ep * SUB + c, placed, 0.0), axis=1, keepdims=True) for c in range(capacity)
    ]

    arrive(0, rec0)
    stat = rec0[0]
    for e in range(n_ep):
        if e:
            stat = stat + rec0[e]
        sum_s[e:e + 1, :] = rec0[e, 0:1, :]
    stat8 = jnp.where(sub == 0, stat[0:1], jnp.where(sub == 1, stat[1:2], 0.0))
    column = stat8.T
    mean = column[:, 0:1] * (1.0 / features)
    spread = column[:, 1:2] * (1.0 / features) - mean * mean
    normed = ((t8_s[...] - mean) * lax.rsqrt(spread + NORM_EPS) * gain_here).astype(BF16)
    gate_rows = lax.dot_general(gate_w, normed, nt, preferred_element_type=F32)
    for j, w in enumerate((wq_v, wk_v)):
        part = jnp.dot(normed, w[...], preferred_element_type=F32)
        part = jnp.where(kind == seq_local, gate_rows[j:j + 1], part)
        for p in range(n_ep):
            msg1[p, :, j * LANES:(j + 1) * LANES] = part[p * SUB:(p + 1) * SUB]
    send(1, "ep", ep_peers, msg1, rec1, True)
    rec1[ep] = msg1[ep]

    mine = (lane == ep * SUB + sub) & (sub < seq_local)
    own_mean = jnp.sum(jnp.where(mine, stat[0:1], 0.0), axis=1, keepdims=True) * (1.0 / features)
    own_square = jnp.sum(jnp.where(mine, stat[1:2], 0.0), axis=1, keepdims=True) * (1.0 / features)
    own_inv = lax.rsqrt(own_square - own_mean * own_mean + NORM_EPS)
    off = lax.dot_general(
        jnp.where(mine, 1.0, 0.0), sum_s[...], nt,
        preferred_element_type=F32, precision=lax.Precision.HIGHEST,
    ) * (1.0 / LANES) - own_mean
    arrive(9, recv)
    for e in range(n_ep):
        arrived = recv[e].astype(F32)
        for j in range(vt):
            piece = arrived[:, j * LANES:(j + 1) * LANES]
            part_s[j, e * SUB:(e + 1) * SUB, :] = piece[:SUB]
            part_s[vt + j, e * SUB:(e + 1) * SUB, :] = piece[SUB:]
    rest_of = []
    for j in range(2 * vt):
        acc = part_s[j, 0:SUB, :]
        for e in range(1, n_ep):
            acc = acc + part_s[j, e * SUB:(e + 1) * SUB, :]
        gain_terms = part_s[j, pl.ds(seq_local, n_ep, SUB), :] + part_s[j, pl.ds(seq_local + 1, n_ep, SUB), :]
        acc = acc + jnp.dot(
            off, gain_terms, preferred_element_type=F32, precision=lax.Precision.HIGHEST
        )
        rest_of.append(jnp.where(sub < seq_local, acc * own_inv, 0.0).astype(BF16).astype(F32))
    value = jnp.concatenate(rest_of[:vt], axis=1)
    outgate = jax.nn.sigmoid(jnp.concatenate(rest_of[vt:], axis=1))
    max8 = jnp.zeros((SUB, LANES), F32)
    for i in range(seq_local):
        max8 = jnp.where(sub == i, max_v[:, i:i + 1], max8)
    head_gain = jnp.concatenate([hg_v[pl.ds(tp * vt + j, 1), :] for j in range(vt)], axis=1)
    wide_p = jnp.concatenate([wp_v[j * LANES:(j + 1) * LANES, :] for j in range(vt)], axis=1)

    arrive(1, rec1)
    sums = rec1[0]
    for e in range(1, n_ep):
        sums = sums + rec1[e]
    in8 = jnp.sum(
        jnp.where(mine, sums[seq_local:seq_local + 1, :LANES], 0.0), axis=1, keepdims=True
    ) + input_bias
    fg8 = jnp.sum(
        jnp.where(mine, sums[seq_local:seq_local + 1, LANES:2 * LANES], 0.0), axis=1, keepdims=True
    ) + forget_bias
    carried = jnp.minimum(fg8, 0.0) - jnp.log1p(jnp.exp(-jnp.abs(fg8))) + max8
    new_max = jnp.maximum(carried, in8)
    keep = jnp.exp(carried - new_max)
    admit = jnp.exp(in8 - new_max)
    across = jnp.sum(jnp.where(sub == iota((SUB, LANES), 1), new_max, 0.0), axis=0, keepdims=True)
    nmax_ref[...] = across[:, :seq_local]
    query = sums[:, :LANES].astype(BF16).astype(F32) * key_size ** (-0.5)
    admitted = admit * sums[:, LANES:2 * LANES].astype(BF16).astype(F32)
    query_t = query.T
    admitted_t = admitted.T
    sub_wide = iota((SUB, value_size), 0)
    readout = jnp.zeros((SUB, value_size), F32)
    for i in range(seq_local):
        nnorm_ref[i] = keep[i:i + 1] * norm_v[i] + admitted[i:i + 1]
        new_cell = keep[i:i + 1, 0:1] * cell_v[i, 0] + admitted_t[:, i:i + 1] * value[i:i + 1, :]
        ncell_ref[i, 0] = new_cell
        read = jnp.sum(query_t[:, i:i + 1] * new_cell, axis=0, keepdims=True)
        readout = jnp.where(sub_wide == i, read, readout)
    head_mean = jnp.mean(readout, axis=1, keepdims=True)
    spread_out = readout - head_mean
    head_var = jnp.mean(spread_out * spread_out, axis=1, keepdims=True)
    mixed = spread_out * lax.rsqrt(head_var + HEAD_EPS) * head_gain * outgate
    mixed = jnp.concatenate([mixed[:, j * LANES:(j + 1) * LANES] for j in range(vt)], axis=0).astype(BF16)
    msg2[...] = mixed

    send(2, "ep", ep_peers, msg2, rec2, False)
    rec2[ep] = mixed
    arrive(2, rec2)
    terms = jnp.dot(
        rec2[...].reshape(n_ep * vt * SUB, LANES), wide_p, preferred_element_type=F32
    )
    for p in range(n_ep):
        term = jnp.zeros((SUB, LANES), F32)
        for j in range(vt):
            start = (p * vt + j) * SUB
            term = term + terms[start:start + SUB, j * LANES:(j + 1) * LANES]
        msg3[p] = term
    send(3, "tp", tp_peers, msg3, rec3, True)
    rec3[tp] = msg3[tp]
    arrive(3, rec3)
    mixer = rec3[0]
    for t in range(1, n_tp):
        mixer = mixer + rec3[t]
    stream16 = (t8_s[pl.ds(pl.multiple_of(tp * SUB, SUB), SUB), :] + mixer).astype(BF16)
    stream = stream16.astype(F32)
    msg4[...] = stream16

    send(4, "ep", ep_peers, msg4, rec4, False)
    rec4[ep] = stream16
    gain2 = gain2_v[...]
    arrive(4, rec4)
    for e in range(n_ep):
        slot_s[e * SUB:(e + 1) * SUB, :] = rec4[e].astype(F32)
    rows_of = [slot_s[pl.ds(r, n_ep, SUB), :] for r in range(seq_local)]
    slots = []
    for c in range(capacity):
        x = chosen[c][0:1, :] * rows_of[0]
        for r in range(1, seq_local):
            x = x + chosen[c][r:r + 1, :] * rows_of[r]
        mean = total(x) * (1.0 / features)
        spread = total(x * x) * (1.0 / features) - mean * mean
        slots.append((x - mean) * lax.rsqrt(spread + NORM_EPS) * gain2)
    slots16 = jnp.concatenate(slots, axis=0).astype(BF16)
    msg5[...] = slots16

    send(5, "tp", tp_peers, msg5, rec5, False)
    rec5[tp] = slots16
    for copy in loads[18:]:
        copy.wait()
    arrive(5, rec5)
    rows_c = capacity * n_ep
    slot_count = capacity * n_tp
    for t in range(n_tp):
        wide_s[t * rows_c:(t + 1) * rows_c, :] = rec5[t].astype(F32)
    x = jnp.concatenate(
        [wide_s[pl.ds(e, slot_count, n_ep), :].astype(BF16) for e in range(n_ep)], axis=1
    )
    gate = jnp.dot(x, eg_v[0], preferred_element_type=F32)
    up = jnp.dot(x, eu_v[0], preferred_element_type=F32)
    active = (jax.nn.silu(gate) * up).astype(BF16)
    down = jnp.dot(active, ed_v[0], preferred_element_type=F32)
    for e in range(n_ep):
        wide_s[pl.ds(e, slot_count, n_ep), :] = down[:, e * LANES:(e + 1) * LANES]
    for t in range(n_tp):
        msg6[t] = wide_s[t * rows_c:(t + 1) * rows_c, :].astype(BF16)
    send(6, "tp", tp_peers, msg6, rec6, True)
    rec6[tp] = msg6[tp]
    slot_s[...] = jnp.zeros_like(slot_s)
    arrive(6, rec6)
    done = rec6[0].astype(F32)
    for t in range(1, n_tp):
        done = done + rec6[t].astype(F32)
    for c in range(capacity):
        slot_s[pl.ds(c, n_ep, SUB), :] = done[c * n_ep:(c + 1) * n_ep]
    for e in range(n_ep):
        msg7[e] = slot_s[e * SUB:(e + 1) * SUB, :].astype(BF16)

    send(7, "ep", ep_peers, msg7, rec7, True)
    rec7[ep] = msg7[ep]
    arrive(7, rec7)
    returned = jnp.concatenate([rec7[e].astype(F32) for e in range(n_ep)], axis=0).astype(BF16)
    lhs = jnp.concatenate(
        [weight_high.astype(F32), weight_mid.astype(F32), weight_low.astype(F32)], axis=0
    )[:, :SUB * n_ep].astype(BF16)
    moe = jnp.dot(lhs, returned, preferred_element_type=F32)
    moe = moe[0:SUB] + moe[SUB:2 * SUB] + moe[2 * SUB:3 * SUB]
    layer16 = (stream + moe).astype(BF16)
    msg8[...] = layer16
    send(8, "tp", tp_peers, msg8, rec8, False)
    rec8[tp] = layer16
    arrive(8, rec8)
    finished = jnp.concatenate([rec8[t].astype(F32) for t in range(n_tp)], axis=0).astype(BF16)
    c8 = iota((seqs, SUB * n_tp), 1)
    unpick = (c8 // SUB) * seq_local + c8 % SUB == iota((seqs, SUB * n_tp), 0)
    unpick = unpick & (c8 % SUB < seq_local)
    out_ref[...] = jnp.dot(unpick.astype(BF16), finished, preferred_element_type=F32).astype(BF16)

    for phase, target in enumerate((rec0, rec1, rec2, rec3, rec4, rec5, rec6, rec7, rec8, recv)):
        drain(phase, target)


def solution(mesh):
    n_ep = mesh.shape["ep"]
    n_tp = mesh.shape["tp"]

    def on_device(*args):
        (
            tokens, first_gain, w_query, w_key, w_value, w_outgate, w_input, w_forget,
            input_bias, forget_bias, head_gain, w_project, cell_state, norm_state, max_state,
            second_gain, routes, route_weight, expert_gate, expert_up, expert_down,
        ) = args
        seq_local = tokens.shape[0] // n_ep
        key_size, value_size = cell_state.shape[2], cell_state.shape[3]
        capacity = 2
        operands = (
            tokens, first_gain.reshape(n_ep, LANES), w_query, w_key, w_value, w_outgate,
            w_input.T, w_forget.T, input_bias.reshape(1, -1), forget_bias.reshape(1, -1),
            head_gain.reshape(-1, LANES), w_project, cell_state, norm_state, max_state.T,
            second_gain.reshape(n_ep, LANES), routes.T, route_weight.T,
            expert_gate, expert_up, expert_down,
        )
        hbm = pl.BlockSpec(memory_space=pltpu.HBM)
        vmem = pl.BlockSpec(memory_space=pltpu.VMEM)
        rows8 = max(SUB * n_ep, LANES)
        vt = value_size // LANES

        def pair(shape_out, shape_in, dtype):
            return [pltpu.VMEM(shape_out, dtype), pltpu.VMEM(shape_in, dtype)]

        messages = (
            pair((2, rows8), (n_ep, 2, rows8), F32)
            + pair((n_ep, 2 * SUB, value_size), (n_ep, 2 * SUB, value_size), BF16)
            + pair((n_ep, SUB, 2 * key_size), (n_ep, SUB, 2 * key_size), F32)
            + pair((vt * SUB, LANES), (n_ep, vt * SUB, LANES), BF16)
            + pair((n_tp, SUB, LANES), (n_tp, SUB, LANES), F32)
            + pair((SUB, LANES), (n_ep, SUB, LANES), BF16)
            + pair((capacity * n_ep, LANES), (n_tp, capacity * n_ep, LANES), BF16)
            + pair((n_tp, capacity * n_ep, LANES), (n_tp, capacity * n_ep, LANES), BF16)
            + pair((n_ep, SUB, LANES), (n_ep, SUB, LANES), BF16)
            + pair((SUB, LANES), (n_tp, SUB, LANES), BF16)
        )
        out, new_cell, new_norm, new_max = pl.pallas_call(
            functools.partial(kernel, n_ep, n_tp, seq_local, key_size, value_size),
            out_shape=(
                jax.ShapeDtypeStruct(tokens.shape, BF16),
                jax.ShapeDtypeStruct(cell_state.shape, F32),
                jax.ShapeDtypeStruct(norm_state.shape, F32),
                jax.ShapeDtypeStruct((1, seq_local), F32),
            ),
            in_specs=[hbm] * len(operands),
            out_specs=(vmem, vmem, vmem, vmem),
            scratch_shapes=[pltpu.VMEM(a.shape, a.dtype) for a in operands]
            + messages
            + [
                pltpu.VMEM((rows8, LANES), F32),
                pltpu.VMEM((2 * vt, rows8, LANES), F32),
                pltpu.VMEM((n_ep, rows8), F32),
                pltpu.VMEM((SUB * n_ep, LANES), F32),
                pltpu.VMEM((n_tp * capacity * n_ep, LANES), F32),
                pltpu.SemaphoreType.DMA((len(operands),)),
                pltpu.SemaphoreType.DMA((10,)),
                pltpu.SemaphoreType.DMA((10,)),
            ],
            compiler_params=pltpu.CompilerParams(
                collective_id=0, has_side_effects=True
            ),
        )(*operands)
        return out, new_cell, new_norm, new_max.T

    placed = (
        P("grp", "ep"), P(), P("ep", "tp"), P("ep", "tp"), P("ep", "tp"), P("ep", "tp"),
        P(), P(), P(), P(), P(), P("tp", "ep"),
        P(("grp", "ep"), "tp", None, None), P(("grp", "ep"), "tp", None), P(("grp", "ep"), "tp"),
        P(), P("grp", None), P("grp", None),
        P("ep", None, "tp"), P("ep", None, "tp"), P("ep", "tp", None),
    )
    return jax.shard_map(
        on_device,
        mesh=mesh,
        in_specs=placed,
        out_specs=(
            P("grp", "ep"),
            P(("grp", "ep"), "tp", None, None),
            P(("grp", "ep"), "tp", None),
            P(("grp", "ep"), "tp"),
        ),
        check_vma=False,
    )
```

time: 234 us -> 114 us (0.49)
  Pallas kernels: 0 us -> 109 us
  starting transfers between devices: 68.5 us -> 0 us
  blocking collectives: 68.3 us -> 0 us
  waiting for transfers between devices: 56.8 us -> 0 us
  other arithmetic: 15.6 us -> 0 us
  local copies, waits for them, and re-layouts: 17.4 us -> 4.55 us
  matrix products: 5.14 us -> 0 us
    pallas_call x0 -> x1, Pallas kernels: none -> 109 us  [on_device(): pl.pallas_call(functools.partial(kernel, n_ep, n_tp, seq_local, key_size,...]
    all_to_all x5 -> x0, starting transfers between devices: 68.5 us -> none  [the longest x4 64.3 us: from_everyone(): lax.all_to_all(jnp.broadcast_to(array[None], (peers, *array.shape)), axis...]
    all_to_all x5 -> x0, waiting for transfers between devices: 56.8 us -> none  [the longest x4 39.9 us: from_everyone(): lax.all_to_all(jnp.broadcast_to(array[None], (peers, *array.shape)), axis...]
    all_to_all x3 -> x0, blocking collectives: 45.9 us -> none  [the longest x1 16.3 us: summed_on_arrival(): lax.all_to_all(blocks, axis, split_axis=0, concat_axis=0, tiled=True)]
    all_gather x1 -> x0, blocking collectives: 22.3 us -> none  [gathered_total(): blocks = lax.all_gather(array, axis)]
    unnamed x1 -> x0, other arithmetic: 11.5 us -> none
    dot_general x12 -> x0, matrix products: 5.14 us -> none  [the longest x6 2.28 us: project_part(): return jnp.dot(normed, weight, preferred_element_type=jnp.float32)]
    dynamic_slice x5 -> x0, local copies, waits for them, and re-layouts: 3.47 us -> none  [the longest x2 1.53 us: row_norm(): lax.dynamic_slice_in_dim(gain_whole, lax.axis_index('ep') * col_count, co...]
  transfers between devices with their start and end apart: 5 -> 0, of which waited for: 5 -> 0; matrix products, arithmetic and copies ran while one was open for 2% -> 0% of each run, Pallas kernels for 0% -> 0%
where the time goes in v1:
time: 114 us
  Pallas kernels  109 us (96%)
  local copies, waits for them, and re-layouts  4.55 us (4%)
    pallas_call x1, Pallas kernels, on_device(): pl.pallas_call(functools.partial(kernel, n_ep, n_tp, seq_local, key_size,...  109 us
    unnamed x8, local copies, waits for them, and re-layouts  4.55 us

profile of v1, /device:TPU:65, one launch (start us, length us, event | category | flops | bytes accessed | tf_op | source)
XLA Modules:
  0.0 114.0 jit_solution(7118411299902153749)
XLA Ops:
  0.6 108.8 %shard_map.228 = (bf16[96,128]{1,0:T(8,128)(2,1)}, f32[6,1,128,256]{3,2,1,0:T(8,128)}, f32[6,1,128]{2,1,0:T(1,128)}, f32[1,6]{1,0:T(1,128)}) custom-call(bf16[96,128]{1,0:T(8,128)(2,1)} %tokens_h.1, f32[16,128]{1,0:T(8,128)} %bitcast.14, bf16[128,128]{1,0:T(8,128)(2,1)} %wq_h.1, bf16[128,128]{1,0:T(8,128)(2,1)} %wk_h.1, bf16[128,256]{1,0:T(8,128)(2,1)} %wv_h.1, ...), custom_call_target="tpu_custom_call" | custom-call | tf_op jit(solution)/shard_map/pallas_call | solution.py:405
  109.4 1.3 %copy.29 = bf16[96,128]{1,0:T(8,128)(2,1)} copy(bf16[96,128]{1,0:T(8,128)(2,1)} %get-tuple-element.16) | data formatting | bytes 49152
  110.8 0.0 copy-start
  110.8 2.1 %copy.30 = f32[6,1,128,256]{3,2,1,0:T(8,128)} copy(f32[6,1,128,256]{3,2,1,0:T(8,128)} %get-tuple-element.17) | data formatting | bytes 1572864
  112.9 0.0 copy-done
  112.9 0.0 copy-start.1
  112.9 0.6 copy.31
  113.5 0.0 copy-done.1
  113.5 0.5 copy.32
Async XLA Ops:
  110.8 2.1 %copy-start = (f32[6,1,128]{2,1,0:T(1,128)S(1)}, f32[6,1,128]{2,1,0:T(1,128)}, u32[]{:S(2)}) copy-start(f32[6,1,128]{2,1,0:T(1,128)} %get-tuple-element.18) | copy-start | bytes 9220
  112.9 0.6 copy-start.1

commit v2 on v1

--- a/solution.py
+++ b/solution.py
@@ -41,17 +41,24 @@
     cell_v, norm_v, max_v, gain2_v, routes_v, rw_v, eg_v, eu_v, ed_v,
     msg0, rec0, msgv, recv, msg1, rec1, msg2, rec2, msg3, rec3, msg4, rec4, msg5, rec5, msg6, rec6, msg7, rec7, msg8, rec8,
     t8_s, part_s, sum_s, slot_s, wide_s,
-    load_sem, send_sem, recv_sem,
+    load_sem, send_sem, recv_sem, known_sem,
 ):
     ep = lax.axis_index("ep")
     tp = lax.axis_index("tp")
     barrier = pltpu.get_barrier_semaphore()
+    rec7[...] = jnp.zeros_like(rec7)
+    rec8[...] = jnp.zeros_like(rec8)
     ep_peers = [lax.rem(ep + d, n_ep) for d in far_first(n_ep)]
     tp_peers = [lax.rem(tp + d, n_tp) for d in far_first(n_tp)]
     for peer in ep_peers:
         pl.semaphore_signal(barrier, inc=1, device_id={"ep": peer}, device_id_type=pl.DeviceIdType.MESH)
-    for peer in tp_peers:
-        pl.semaphore_signal(barrier, inc=1, device_id={"tp": peer}, device_id_type=pl.DeviceIdType.MESH)
+
+    def tell(sem, reach):
+        for d in (reach, n_tp - reach):
+            peer = lax.rem(tp + d, n_tp)
+            pl.semaphore_signal(sem, inc=1, device_id={"tp": peer}, device_id_type=pl.DeviceIdType.MESH)
+
+    tell(barrier, 1)
 
     sources = (
         tokens_h, gain1_h, wq_h, wk_h, wv_h, wo_h, win_h, wfg_h, ib_h, fb_h, hg_h, wp_h,
@@ -67,25 +74,26 @@
     for copy in loads:
         copy.start()
 
-    def send(phase, axis, peers, source, target, each):
+    def send(phase, axis, peers, source, target, each, used=None):
         me = ep if axis == "ep" else tp
+        used = pl.ds(0, target.shape[1] if used is None else used)
         for peer in peers:
             pltpu.make_async_remote_copy(
-                src_ref=source.at[peer] if each else source,
-                dst_ref=target.at[me],
+                src_ref=source.at[peer, used] if each else source.at[used],
+                dst_ref=target.at[me, used],
                 send_sem=send_sem.at[phase],
                 recv_sem=recv_sem.at[phase],
                 device_id={axis: peer},
                 device_id_type=pl.DeviceIdType.MESH,
             ).start()
 
-    def arrive(phase, target):
-        others = target.at[pl.ds(0, target.shape[0] - 1)]
-        pltpu.make_async_copy(others, others, recv_sem.at[phase]).wait()
-
-    def drain(phase, target):
-        others = target.at[pl.ds(0, target.shape[0] - 1)]
-        pltpu.make_async_copy(others, others, send_sem.at[phase]).wait()
+    def settle(sem, target, used):
+        used = target.shape[1] if used is None else used
+        others = target.at[pl.ds(0, target.shape[0] - 1), pl.ds(0, used)]
+        pltpu.make_async_copy(others, others, sem).wait()
+
+    def arrive(phase, target, used=None):
+        settle(recv_sem.at[phase], target, used)
 
     rows8 = max(SUB * n_ep, LANES)
     seqs = n_ep * seq_local
@@ -134,11 +142,16 @@
                 [part_s[j, rows, :], part_s[vt + j, rows, :]], axis=0
             ).astype(BF16)
 
-    pl.semaphore_wait(barrier, len(ep_peers) + len(tp_peers))
+    pl.semaphore_wait(barrier, len(ep_peers) + 2)
+    rounds = [1]
+    while 2 * rounds[-1] < n_tp // 2:
+        rounds.append(2 * rounds[-1])
     send(0, "ep", ep_peers, msg0, rec0, False)
     send(9, "ep", ep_peers, msgv, recv, True)
     rec0[ep] = msg0[...]
     recv[ep] = msgv[ep]
+
+    tell(known_sem.at[0], rounds[0])
 
     for copy in loads[6:18]:
         copy.wait()
@@ -178,6 +191,9 @@
         jnp.sum(jnp.where(lane == ep * SUB + c, placed, 0.0), axis=1, keepdims=True) for c in range(capacity)
     ]
 
+    if len(rounds) > 1:
+        pl.semaphore_wait(known_sem.at[0], 2)
+        tell(known_sem.at[1], rounds[1])
     arrive(0, rec0)
     stat = rec0[0]
     for e in range(n_ep):
@@ -195,7 +211,8 @@
         part = jnp.where(kind == seq_local, gate_rows[j:j + 1], part)
         for p in range(n_ep):
             msg1[p, :, j * LANES:(j + 1) * LANES] = part[p * SUB:(p + 1) * SUB]
-    send(1, "ep", ep_peers, msg1, rec1, True)
+    q_rows = seq_local + 1
+    send(1, "ep", ep_peers, msg1, rec1, True, q_rows)
     rec1[ep] = msg1[ep]
 
     mine = (lane == ep * SUB + sub) & (sub < seq_local)
@@ -206,6 +223,9 @@
         jnp.where(mine, 1.0, 0.0), sum_s[...], nt,
         preferred_element_type=F32, precision=lax.Precision.HIGHEST,
     ) * (1.0 / LANES) - own_mean
+    if len(rounds) > 2:
+        pl.semaphore_wait(known_sem.at[1], 2)
+        tell(known_sem.at[2], rounds[2])
     arrive(9, recv)
     for e in range(n_ep):
         arrived = recv[e].astype(F32)
@@ -231,7 +251,7 @@
     head_gain = jnp.concatenate([hg_v[pl.ds(tp * vt + j, 1), :] for j in range(vt)], axis=1)
     wide_p = jnp.concatenate([wp_v[j * LANES:(j + 1) * LANES, :] for j in range(vt)], axis=1)
 
-    arrive(1, rec1)
+    arrive(1, rec1, q_rows)
     sums = rec1[0]
     for e in range(1, n_ep):
         sums = sums + rec1[e]
@@ -247,6 +267,7 @@
     admit = jnp.exp(in8 - new_max)
     across = jnp.sum(jnp.where(sub == iota((SUB, LANES), 1), new_max, 0.0), axis=0, keepdims=True)
     nmax_ref[...] = across[:, :seq_local]
+    sums = jnp.where(iota((SUB, 2 * LANES), 0) < seq_local, sums, 0.0)
     query = sums[:, :LANES].astype(BF16).astype(F32) * key_size ** (-0.5)
     admitted = admit * sums[:, LANES:2 * LANES].astype(BF16).astype(F32)
     query_t = query.T
@@ -277,21 +298,24 @@
         for j in range(vt):
             start = (p * vt + j) * SUB
             term = term + terms[start:start + SUB, j * LANES:(j + 1) * LANES]
-        msg3[p] = term
-    send(3, "tp", tp_peers, msg3, rec3, True)
+        msg3[p] = term.astype(BF16)
+    last = len(rounds) - 1
+    pl.semaphore_wait(known_sem.at[last], 2)
+    send(3, "tp", tp_peers, msg3, rec3, True, seq_local)
     rec3[tp] = msg3[tp]
-    arrive(3, rec3)
-    mixer = rec3[0]
+    arrive(3, rec3, seq_local)
+    mixer = rec3[0].astype(F32)
     for t in range(1, n_tp):
-        mixer = mixer + rec3[t]
+        mixer = mixer + rec3[t].astype(F32)
+    mixer = jnp.where(sub < seq_local, mixer, 0.0)
     stream16 = (t8_s[pl.ds(pl.multiple_of(tp * SUB, SUB), SUB), :] + mixer).astype(BF16)
     stream = stream16.astype(F32)
     msg4[...] = stream16
 
-    send(4, "ep", ep_peers, msg4, rec4, False)
+    send(4, "ep", ep_peers, msg4, rec4, False, seq_local)
     rec4[ep] = stream16
     gain2 = gain2_v[...]
-    arrive(4, rec4)
+    arrive(4, rec4, seq_local)
     for e in range(n_ep):
         slot_s[e * SUB:(e + 1) * SUB, :] = rec4[e].astype(F32)
     rows_of = [slot_s[pl.ds(r, n_ep, SUB), :] for r in range(seq_local)]
@@ -338,9 +362,9 @@
     for e in range(n_ep):
         msg7[e] = slot_s[e * SUB:(e + 1) * SUB, :].astype(BF16)
 
-    send(7, "ep", ep_peers, msg7, rec7, True)
+    send(7, "ep", ep_peers, msg7, rec7, True, capacity)
     rec7[ep] = msg7[ep]
-    arrive(7, rec7)
+    arrive(7, rec7, capacity)
     returned = jnp.concatenate([rec7[e].astype(F32) for e in range(n_ep)], axis=0).astype(BF16)
     lhs = jnp.concatenate(
         [weight_high.astype(F32), weight_mid.astype(F32), weight_low.astype(F32)], axis=0
@@ -349,17 +373,28 @@
     moe = moe[0:SUB] + moe[SUB:2 * SUB] + moe[2 * SUB:3 * SUB]
     layer16 = (stream + moe).astype(BF16)
     msg8[...] = layer16
-    send(8, "tp", tp_peers, msg8, rec8, False)
+    send(8, "tp", tp_peers, msg8, rec8, False, seq_local)
     rec8[tp] = layer16
-    arrive(8, rec8)
+    arrive(8, rec8, seq_local)
     finished = jnp.concatenate([rec8[t].astype(F32) for t in range(n_tp)], axis=0).astype(BF16)
     c8 = iota((seqs, SUB * n_tp), 1)
     unpick = (c8 // SUB) * seq_local + c8 % SUB == iota((seqs, SUB * n_tp), 0)
     unpick = unpick & (c8 % SUB < seq_local)
     out_ref[...] = jnp.dot(unpick.astype(BF16), finished, preferred_element_type=F32).astype(BF16)
 
+    used_rows = (None, q_rows, None, seq_local, seq_local, None, None, capacity, seq_local, None)
     for phase, target in enumerate((rec0, rec1, rec2, rec3, rec4, rec5, rec6, rec7, rec8, recv)):
-        drain(phase, target)
+        settle(send_sem.at[phase], target, used_rows[phase])
+
+
+def write_out(*refs):
+    *refs, sem = refs
+    count = len(refs) // 2
+    copies = [pltpu.make_async_copy(refs[i], refs[count + i], sem.at[i]) for i in range(count)]
+    for copy in copies:
+        copy.start()
+    for copy in copies:
+        copy.wait()
 
 
 def solution(mesh):
@@ -382,6 +417,12 @@
             second_gain.reshape(n_ep, LANES), routes.T, route_weight.T,
             expert_gate, expert_up, expert_down,
         )
+        results = (
+            jax.ShapeDtypeStruct(tokens.shape, BF16),
+            jax.ShapeDtypeStruct(cell_state.shape, F32),
+            jax.ShapeDtypeStruct(norm_state.shape, F32),
+            jax.ShapeDtypeStruct((1, seq_local), F32),
+        )
         hbm = pl.BlockSpec(memory_space=pltpu.HBM)
         vmem = pl.BlockSpec(memory_space=pltpu.VMEM)
         rows8 = max(SUB * n_ep, LANES)
@@ -395,21 +436,16 @@
             + pair((n_ep, 2 * SUB, value_size), (n_ep, 2 * SUB, value_size), BF16)
             + pair((n_ep, SUB, 2 * key_size), (n_ep, SUB, 2 * key_size), F32)
             + pair((vt * SUB, LANES), (n_ep, vt * SUB, LANES), BF16)
-            + pair((n_tp, SUB, LANES), (n_tp, SUB, LANES), F32)
+            + pair((n_tp, SUB, LANES), (n_tp, SUB, LANES), BF16)
             + pair((SUB, LANES), (n_ep, SUB, LANES), BF16)
             + pair((capacity * n_ep, LANES), (n_tp, capacity * n_ep, LANES), BF16)
             + pair((n_tp, capacity * n_ep, LANES), (n_tp, capacity * n_ep, LANES), BF16)
             + pair((n_ep, SUB, LANES), (n_ep, SUB, LANES), BF16)
             + pair((SUB, LANES), (n_tp, SUB, LANES), BF16)
         )
-        out, new_cell, new_norm, new_max = pl.pallas_call(
+        held = pl.pallas_call(
             functools.partial(kernel, n_ep, n_tp, seq_local, key_size, value_size),
-            out_shape=(
-                jax.ShapeDtypeStruct(tokens.shape, BF16),
-                jax.ShapeDtypeStruct(cell_state.shape, F32),
-                jax.ShapeDtypeStruct(norm_state.shape, F32),
-                jax.ShapeDtypeStruct((1, seq_local), F32),
-            ),
+            out_shape=tuple(pltpu.VMEM(r.shape, r.dtype) for r in results),
             in_specs=[hbm] * len(operands),
             out_specs=(vmem, vmem, vmem, vmem),
             scratch_shapes=[pltpu.VMEM(a.shape, a.dtype) for a in operands]
@@ -423,11 +459,20 @@
                 pltpu.SemaphoreType.DMA((len(operands),)),
                 pltpu.SemaphoreType.DMA((10,)),
                 pltpu.SemaphoreType.DMA((10,)),
+                pltpu.SemaphoreType.REGULAR((3,)),
             ],
             compiler_params=pltpu.CompilerParams(
                 collective_id=0, has_side_effects=True
             ),
         )(*operands)
+        out, new_cell, new_norm, new_max = pl.pallas_call(
+            write_out,
+            out_shape=results,
+            in_specs=[pl.BlockSpec(memory_space=pl.ANY)] * len(results),
+            out_specs=(hbm,) * len(results),
+            scratch_shapes=[pltpu.SemaphoreType.DMA((len(results),))],
+            compiler_params=pltpu.CompilerParams(vmem_limit_bytes=1024 * 1024),
+        )(*held)
         return out, new_cell, new_norm, new_max.T
 
     placed = (

time: 114 us -> 109 us (0.956)
  local copies, waits for them, and re-layouts: 4.55 us -> 0 us
    unnamed x8 -> x0, local copies, waits for them, and re-layouts: 4.55 us -> none
    pallas_call x1, Pallas kernels: 109 us -> 107 us  [on_device(): pl.pallas_call(functools.partial(kernel, n_ep, n_tp, seq_local, key_size,...]
where the time goes in v2:
time: 109 us
  Pallas kernels  108 us (99%)
    pallas_call x1, Pallas kernels, on_device(): pl.pallas_call(functools.partial(kernel, n_ep, n_tp, seq_local, key_size,...  107 us

profile of v2, /device:TPU:65, one launch (start us, length us, event | category | flops | bytes accessed | tf_op | source)
XLA Modules:
  0.0 108.5 jit_solution(8791859313108784031)
XLA Ops:
  0.6 107.0 %shard_map.228 = (bf16[96,128]{1,0:T(8,128)(2,1)S(1)}, f32[6,1,128,256]{3,2,1,0:T(8,128)S(1)}, f32[6,1,128]{2,1,0:T(1,128)S(1)}, f32[1,6]{1,0:T(1,128)S(1)}) custom-call(bf16[96,128]{1,0:T(8,128)(2,1)} %tokens_h.1, f32[16,128]{1,0:T(8,128)} %bitcast.14, bf16[128,128]{1,0:T(8,128)(2,1)} %wq_h.1, bf16[128,128]{1,0:T(8,128)(2,1)} %wk_h.1, ...), custom_call_target="tpu_custom_call" | custom-call | tf_op jit(solution)/shard_map/pallas_call | solution.py:446
  107.6 0.9 shard_map.229

commit v3 on v2

--- a/solution.py
+++ b/solution.py
@@ -40,19 +40,17 @@
     tokens_v, gain1_v, wq_v, wk_v, wv_v, wo_v, win_v, wfg_v, ib_v, fb_v, hg_v, wp_v,
     cell_v, norm_v, max_v, gain2_v, routes_v, rw_v, eg_v, eu_v, ed_v,
     msg0, rec0, msgv, recv, msg1, rec1, msg2, rec2, msg3, rec3, msg4, rec4, msg5, rec5, msg6, rec6, msg7, rec7, msg8, rec8,
-    t8_s, part_s, sum_s, slot_s, wide_s,
-    load_sem, send_sem, recv_sem, known_sem,
+    table, t8_s, part_s, sum_s, slot_s, wide_s,
+    load_sem, send_sem, recv_sem, known_sem, stat_send, stat_recv,
 ):
     ep = lax.axis_index("ep")
     tp = lax.axis_index("tp")
     barrier = pltpu.get_barrier_semaphore()
     rec7[...] = jnp.zeros_like(rec7)
     rec8[...] = jnp.zeros_like(rec8)
+    table[...] = jnp.zeros_like(table)
     ep_peers = [lax.rem(ep + d, n_ep) for d in far_first(n_ep)]
     tp_peers = [lax.rem(tp + d, n_tp) for d in far_first(n_tp)]
-    for peer in ep_peers:
-        pl.semaphore_signal(barrier, inc=1, device_id={"ep": peer}, device_id_type=pl.DeviceIdType.MESH)
-
     def tell(sem, reach):
         for d in (reach, n_tp - reach):
             peer = lax.rem(tp + d, n_tp)
@@ -142,13 +140,44 @@
                 [part_s[j, rows, :], part_s[vt + j, rows, :]], axis=0
             ).astype(BF16)
 
-    pl.semaphore_wait(barrier, len(ep_peers) + 2)
+    @pl.when(ep == 0)
+    def _():
+        pl.semaphore_wait(barrier, 2)
+
+    @pl.when(ep > 0)
+    def _():
+        pl.semaphore_wait(barrier, 3)
+
+    above = lax.rem(ep + 1, n_ep)
+
+    @pl.when(ep < n_ep - 1)
+    def _():
+        pl.semaphore_signal(barrier, inc=1, device_id={"ep": above}, device_id_type=pl.DeviceIdType.MESH)
+
     rounds = [1]
     while 2 * rounds[-1] < n_tp // 2:
         rounds.append(2 * rounds[-1])
-    send(0, "ep", ep_peers, msg0, rec0, False)
-    send(9, "ep", ep_peers, msgv, recv, True)
-    rec0[ep] = msg0[...]
+    def statistics_to(peer):
+        return pltpu.make_async_remote_copy(
+            src_ref=msg0, dst_ref=rec0.at[ep], send_sem=stat_send.at[peer], recv_sem=stat_recv.at[ep],
+            device_id={"ep": peer}, device_id_type=pl.DeviceIdType.MESH,
+        )
+
+    def terms_to(peer):
+        return pltpu.make_async_remote_copy(
+            src_ref=msgv.at[peer], dst_ref=recv.at[ep], send_sem=send_sem.at[9], recv_sem=recv_sem.at[9],
+            device_id={"ep": peer}, device_id_type=pl.DeviceIdType.MESH,
+        )
+
+    table_up = pltpu.make_async_remote_copy(
+        src_ref=table, dst_ref=table, send_sem=send_sem.at[0], recv_sem=recv_sem.at[0],
+        device_id={"ep": above}, device_id_type=pl.DeviceIdType.MESH,
+    )
+    for make in (statistics_to, terms_to):
+        for d in far_first(n_ep):
+            @pl.when(ep >= d)
+            def _(make=make, d=d):
+                make(lax.rem(ep + n_ep - d, n_ep)).start()
     recv[ep] = msgv[ep]
 
     tell(known_sem.at[0], rounds[0])
@@ -194,12 +223,27 @@
     if len(rounds) > 1:
         pl.semaphore_wait(known_sem.at[0], 2)
         tell(known_sem.at[1], rounds[1])
-    arrive(0, rec0)
-    stat = rec0[0]
+    @pl.when(ep > 0)
+    def _():
+        table_up.wait_recv()
+
+    table[ep] = msg0[...]
+    for e in range(1, n_ep):
+        @pl.when(e > ep)
+        def _(e=e):
+            pltpu.make_async_copy(rec0.at[e], rec0.at[e], stat_recv.at[e]).wait()
+
+            @pl.when(e == ep + 1)
+            def _():
+                table_up.start()
+
+            terms_to(e).start()
+
+    stat = jnp.zeros((2, rows8), F32)
     for e in range(n_ep):
-        if e:
-            stat = stat + rec0[e]
-        sum_s[e:e + 1, :] = rec0[e, 0:1, :]
+        theirs = jnp.where(e <= ep, table[e], rec0[e])
+        stat = stat + theirs
+        sum_s[e:e + 1, :] = theirs[0:1]
     stat8 = jnp.where(sub == 0, stat[0:1], jnp.where(sub == 1, stat[1:2], 0.0))
     column = stat8.T
     mean = column[:, 0:1] * (1.0 / features)
@@ -382,9 +426,18 @@
     unpick = unpick & (c8 % SUB < seq_local)
     out_ref[...] = jnp.dot(unpick.astype(BF16), finished, preferred_element_type=F32).astype(BF16)
 
-    used_rows = (None, q_rows, None, seq_local, seq_local, None, None, capacity, seq_local, None)
-    for phase, target in enumerate((rec0, rec1, rec2, rec3, rec4, rec5, rec6, rec7, rec8, recv)):
-        settle(send_sem.at[phase], target, used_rows[phase])
+    @pl.when(ep < n_ep - 1)
+    def _():
+        table_up.wait_send()
+
+    for e in range(n_ep - 1):
+        @pl.when(e < ep)
+        def _(e=e):
+            pltpu.make_async_copy(msg0, msg0, stat_send.at[e]).wait()
+
+    used_rows = (q_rows, None, seq_local, seq_local, None, None, capacity, seq_local, None)
+    for phase, target in enumerate((rec1, rec2, rec3, rec4, rec5, rec6, rec7, rec8, recv), 1):
+        settle(send_sem.at[phase], target, used_rows[phase - 1])
 
 
 def write_out(*refs):
@@ -451,6 +504,7 @@
             scratch_shapes=[pltpu.VMEM(a.shape, a.dtype) for a in operands]
             + messages
             + [
+                pltpu.VMEM((n_ep, 2, rows8), F32),
                 pltpu.VMEM((rows8, LANES), F32),
                 pltpu.VMEM((2 * vt, rows8, LANES), F32),
                 pltpu.VMEM((n_ep, rows8), F32),
@@ -460,6 +514,8 @@
                 pltpu.SemaphoreType.DMA((10,)),
                 pltpu.SemaphoreType.DMA((10,)),
                 pltpu.SemaphoreType.REGULAR((3,)),
+                pltpu.SemaphoreType.DMA((n_ep,)),
+                pltpu.SemaphoreType.DMA((n_ep,)),
             ],
             compiler_params=pltpu.CompilerParams(
                 collective_id=0, has_side_effects=True

time: 109 us -> 144 us (1.32)
  Pallas kernels: 108 us -> 143 us
    pallas_call x1, Pallas kernels: 107 us -> 142 us  [on_device(): pl.pallas_call(functools.partial(kernel, n_ep, n_tp, seq_local, key_size,...]
where the time goes in v3:
time: 144 us; the launch traced here: 143 us
  Pallas kernels  143 us (99%)
    pallas_call x1, Pallas kernels, on_device(): pl.pallas_call(functools.partial(kernel, n_ep, n_tp, seq_local, key_size,...  142 us

profile of v3, /device:TPU:65, one launch (start us, length us, event | category | flops | bytes accessed | tf_op | source)
XLA Modules:
  0.0 143.4 jit_solution(14534443708616457013)
XLA Ops:
  0.6 141.9 %shard_map.228 = (bf16[96,128]{1,0:T(8,128)(2,1)S(1)}, f32[6,1,128,256]{3,2,1,0:T(8,128)S(1)}, f32[6,1,128]{2,1,0:T(1,128)S(1)}, f32[1,6]{1,0:T(1,128)S(1)}) custom-call(bf16[96,128]{1,0:T(8,128)(2,1)} %tokens_h.1, f32[16,128]{1,0:T(8,128)} %bitcast.14, bf16[128,128]{1,0:T(8,128)(2,1)} %wq_h.1, bf16[128,128]{1,0:T(8,128)(2,1)} %wk_h.1, ...), custom_call_target="tpu_custom_call" | custom-call | tf_op jit(solution)/shard_map/pallas_call | solution.py:499
  142.5 0.9 shard_map.229

commit v4 on v2

--- a/solution.py
+++ b/solution.py
@@ -40,19 +40,17 @@
     tokens_v, gain1_v, wq_v, wk_v, wv_v, wo_v, win_v, wfg_v, ib_v, fb_v, hg_v, wp_v,
     cell_v, norm_v, max_v, gain2_v, routes_v, rw_v, eg_v, eu_v, ed_v,
     msg0, rec0, msgv, recv, msg1, rec1, msg2, rec2, msg3, rec3, msg4, rec4, msg5, rec5, msg6, rec6, msg7, rec7, msg8, rec8,
-    t8_s, part_s, sum_s, slot_s, wide_s,
-    load_sem, send_sem, recv_sem, known_sem,
+    table, t8_s, part_s, sum_s, slot_s, wide_s,
+    load_sem, send_sem, recv_sem, known_sem, stat_send, stat_recv,
 ):
     ep = lax.axis_index("ep")
     tp = lax.axis_index("tp")
     barrier = pltpu.get_barrier_semaphore()
     rec7[...] = jnp.zeros_like(rec7)
     rec8[...] = jnp.zeros_like(rec8)
+    table[...] = jnp.zeros_like(table)
     ep_peers = [lax.rem(ep + d, n_ep) for d in far_first(n_ep)]
     tp_peers = [lax.rem(tp + d, n_tp) for d in far_first(n_tp)]
-    for peer in ep_peers:
-        pl.semaphore_signal(barrier, inc=1, device_id={"ep": peer}, device_id_type=pl.DeviceIdType.MESH)
-
     def tell(sem, reach):
         for d in (reach, n_tp - reach):
             peer = lax.rem(tp + d, n_tp)
@@ -73,6 +71,25 @@
     ]
     for copy in loads:
         copy.start()
+
+    place = lax.rem(ep + n_ep - 1, n_ep)
+
+    def at_place(q):
+        return lax.rem(q + 1, n_ep)
+
+    @pl.when(place == 0)
+    def _():
+        pl.semaphore_wait(barrier, 2)
+
+    @pl.when((place > 0) & (place < n_ep - 1))
+    def _():
+        pl.semaphore_wait(barrier, 3)
+
+    @pl.when(place < n_ep - 1)
+    def _():
+        pl.semaphore_signal(
+            barrier, inc=1, device_id={"ep": at_place(place + 1)}, device_id_type=pl.DeviceIdType.MESH
+        )
 
     def send(phase, axis, peers, source, target, each, used=None):
         me = ep if axis == "ep" else tp
@@ -104,8 +121,7 @@
     kt = key_size // LANES
     vt = value_size // LANES
 
-    for copy in loads[:6]:
-        copy.wait()
+    loads[0].wait()
     r8 = iota((rows8, seqs), 0)
     pick = ((r8 // SUB) * seq_local + r8 % SUB == iota((rows8, seqs), 1)) & (r8 % SUB < seq_local)
     t8 = jnp.dot(pick.astype(BF16), tokens_v[...], preferred_element_type=F32)
@@ -115,6 +131,34 @@
     row_square = jnp.sum(t8 * t8, axis=1, keepdims=True)
     stats = jnp.where(wide_lane == 0, row_sum, jnp.where(wide_lane == 1, row_square, 0.0)).T
     msg0[...] = stats[0:2]
+
+    @pl.when(place == n_ep - 1)
+    def _():
+        pl.semaphore_wait(barrier, 3)
+
+    def statistics_to(q):
+        return pltpu.make_async_remote_copy(
+            src_ref=msg0, dst_ref=rec0.at[place], send_sem=stat_send.at[q], recv_sem=stat_recv.at[place],
+            device_id={"ep": at_place(q)}, device_id_type=pl.DeviceIdType.MESH,
+        )
+
+    def terms_to(q):
+        return pltpu.make_async_remote_copy(
+            src_ref=msgv.at[at_place(q)], dst_ref=recv.at[place],
+            send_sem=send_sem.at[9], recv_sem=recv_sem.at[9],
+            device_id={"ep": at_place(q)}, device_id_type=pl.DeviceIdType.MESH,
+        )
+
+    def to_those_below(make):
+        def step(q, carry):
+            make(q).start()
+            return carry
+
+        lax.fori_loop(0, place, step, 0)
+
+    to_those_below(statistics_to)
+    for copy in loads[1:6]:
+        copy.wait()
     gain_here = gain1_v[pl.ds(ep, 1), :]
     gain_high = gain_here.astype(BF16).astype(F32)
     kind = iota((rows8, LANES), 0) % SUB
@@ -142,15 +186,15 @@
                 [part_s[j, rows, :], part_s[vt + j, rows, :]], axis=0
             ).astype(BF16)
 
-    pl.semaphore_wait(barrier, len(ep_peers) + 2)
     rounds = [1]
     while 2 * rounds[-1] < n_tp // 2:
         rounds.append(2 * rounds[-1])
-    send(0, "ep", ep_peers, msg0, rec0, False)
-    send(9, "ep", ep_peers, msgv, recv, True)
-    rec0[ep] = msg0[...]
-    recv[ep] = msgv[ep]
-
+    to_those_below(terms_to)
+    recv[place] = msgv[ep]
+    table_up = pltpu.make_async_remote_copy(
+        src_ref=table, dst_ref=table, send_sem=send_sem.at[0], recv_sem=recv_sem.at[0],
+        device_id={"ep": at_place(place + 2)}, device_id_type=pl.DeviceIdType.MESH,
+    )
     tell(known_sem.at[0], rounds[0])
 
     for copy in loads[6:18]:
@@ -194,12 +238,43 @@
     if len(rounds) > 1:
         pl.semaphore_wait(known_sem.at[0], 2)
         tell(known_sem.at[1], rounds[1])
-    arrive(0, rec0)
-    stat = rec0[0]
+    def statistics_from(q):
+        pltpu.make_async_copy(rec0.at[q], rec0.at[q], stat_recv.at[q]).wait()
+
+    @pl.when(place < n_ep - 1)
+    def _():
+        statistics_from(place + 1)
+        statistics_to(place + 1).start()
+        terms_to(place + 1).start()
+
+    @pl.when(place > 1)
+    def _():
+        table_up.wait_recv()
+
+    @pl.when(place > 0)
+    def _():
+        statistics_from(place - 1)
+        table[place - 1] = rec0[place - 1]
+
+    table[place] = msg0[...]
+
+    @pl.when(place < n_ep - 2)
+    def _():
+        statistics_from(place + 2)
+        table_up.start()
+        terms_to(place + 2).start()
+
+    def from_above(q, carry):
+        statistics_from(q)
+        terms_to(q).start()
+        return carry
+
+    lax.fori_loop(place + 3, n_ep, from_above, 0)
+    stat = jnp.zeros((2, rows8), F32)
     for e in range(n_ep):
-        if e:
-            stat = stat + rec0[e]
-        sum_s[e:e + 1, :] = rec0[e, 0:1, :]
+        theirs = jnp.where(e <= place, table[e], rec0[e])
+        stat = stat + theirs
+        sum_s[e:e + 1, :] = theirs[0:1]
     stat8 = jnp.where(sub == 0, stat[0:1], jnp.where(sub == 1, stat[1:2], 0.0))
     column = stat8.T
     mean = column[:, 0:1] * (1.0 / features)
@@ -382,9 +457,23 @@
     unpick = unpick & (c8 % SUB < seq_local)
     out_ref[...] = jnp.dot(unpick.astype(BF16), finished, preferred_element_type=F32).astype(BF16)
 
-    used_rows = (None, q_rows, None, seq_local, seq_local, None, None, capacity, seq_local, None)
-    for phase, target in enumerate((rec0, rec1, rec2, rec3, rec4, rec5, rec6, rec7, rec8, recv)):
-        settle(send_sem.at[phase], target, used_rows[phase])
+    @pl.when(place < n_ep - 2)
+    def _():
+        table_up.wait_send()
+
+    def statistics_left(q, carry):
+        pltpu.make_async_copy(msg0, msg0, stat_send.at[q]).wait()
+        return carry
+
+    lax.fori_loop(0, place, statistics_left, 0)
+
+    @pl.when(place < n_ep - 1)
+    def _():
+        statistics_left(place + 1, 0)
+
+    used_rows = (q_rows, None, seq_local, seq_local, None, None, capacity, seq_local, None)
+    for phase, target in enumerate((rec1, rec2, rec3, rec4, rec5, rec6, rec7, rec8, recv), 1):
+        settle(send_sem.at[phase], target, used_rows[phase - 1])
 
 
 def write_out(*refs):
@@ -451,6 +540,7 @@
             scratch_shapes=[pltpu.VMEM(a.shape, a.dtype) for a in operands]
             + messages
             + [
+                pltpu.VMEM((n_ep, 2, rows8), F32),
                 pltpu.VMEM((rows8, LANES), F32),
                 pltpu.VMEM((2 * vt, rows8, LANES), F32),
                 pltpu.VMEM((n_ep, rows8), F32),
@@ -460,6 +550,8 @@
                 pltpu.SemaphoreType.DMA((10,)),
                 pltpu.SemaphoreType.DMA((10,)),
                 pltpu.SemaphoreType.REGULAR((3,)),
+                pltpu.SemaphoreType.DMA((n_ep,)),
+                pltpu.SemaphoreType.DMA((n_ep,)),
             ],
             compiler_params=pltpu.CompilerParams(
                 collective_id=0, has_side_effects=True

time: 109 us -> 107 us (0.982)
    pallas_call x1, Pallas kernels: 107 us -> 106 us  [on_device(): pl.pallas_call(functools.partial(kernel, n_ep, n_tp, seq_local, key_size,...]
where the time goes in v4:
time: 107 us
  Pallas kernels  107 us (100%)
    pallas_call x1, Pallas kernels, on_device(): pl.pallas_call(functools.partial(kernel, n_ep, n_tp, seq_local, key_size,...  106 us

profile of v4, /device:TPU:65, one launch (start us, length us, event | category | flops | bytes accessed | tf_op | source)
XLA Modules:
  0.0 107.3 jit_solution(9444304745625694808)
XLA Ops:
  0.6 105.7 %shard_map.228 = (bf16[96,128]{1,0:T(8,128)(2,1)S(1)}, f32[6,1,128,256]{3,2,1,0:T(8,128)S(1)}, f32[6,1,128]{2,1,0:T(1,128)S(1)}, f32[1,6]{1,0:T(1,128)S(1)}) custom-call(bf16[96,128]{1,0:T(8,128)(2,1)} %tokens_h.1, f32[16,128]{1,0:T(8,128)} %bitcast.14, bf16[128,128]{1,0:T(8,128)(2,1)} %wq_h.1, bf16[128,128]{1,0:T(8,128)(2,1)} %wk_h.1, ...), custom_call_target="tpu_custom_call" | custom-call | tf_op jit(solution)/shard_map/pallas_call | solution.py:535
  106.3 0.9 shard_map.229

commit v5 on v4

--- a/solution.py
+++ b/solution.py
@@ -36,41 +36,45 @@
     n_ep, n_tp, seq_local, key_size, value_size,
     tokens_h, gain1_h, wq_h, wk_h, wv_h, wo_h, win_h, wfg_h, ib_h, fb_h, hg_h, wp_h,
     cell_h, norm_h, max_h, gain2_h, routes_h, rw_h, eg_h, eu_h, ed_h,
-    out_ref, ncell_ref, nnorm_ref, nmax_ref,
+    rec8, ncell_ref, nnorm_ref, nmax_ref,
     tokens_v, gain1_v, wq_v, wk_v, wv_v, wo_v, win_v, wfg_v, ib_v, fb_v, hg_v, wp_v,
     cell_v, norm_v, max_v, gain2_v, routes_v, rw_v, eg_v, eu_v, ed_v,
-    msg0, rec0, msgv, recv, msg1, rec1, msg2, rec2, msg3, rec3, msg4, rec4, msg5, rec5, msg6, rec6, msg7, rec7, msg8, rec8,
+    msg0, rec0, msgv, recv, msg1, rec1, msg2, rec2, msg3, rec3, msg4, rec4, msg5, rec5, msg6, rec6, msg7, rec7, msg8,
     table, t8_s, part_s, sum_s, slot_s, wide_s,
     load_sem, send_sem, recv_sem, known_sem, stat_send, stat_recv,
 ):
     ep = lax.axis_index("ep")
     tp = lax.axis_index("tp")
+    sources = (
+        tokens_h, gain1_h, wq_h, wk_h, wv_h, wo_h, win_h, wfg_h, ib_h, fb_h, hg_h, wp_h,
+        cell_h, norm_h, max_h, gain2_h, routes_h, rw_h, eg_h, eu_h, ed_h,
+    )
+    targets = (
+        tokens_v, gain1_v, wq_v, wk_v, wv_v, wo_v, win_v, wfg_v, ib_v, fb_v, hg_v, wp_v,
+        cell_v, norm_v, max_v, gain2_v, routes_v, rw_v, eg_v, eu_v, ed_v,
+    )
+    loads = [
+        pltpu.make_async_copy(s, t, load_sem.at[i]) for i, (s, t) in enumerate(zip(sources, targets))
+    ]
+    for copy in loads[:6]:
+        copy.start()
     barrier = pltpu.get_barrier_semaphore()
     rec7[...] = jnp.zeros_like(rec7)
     rec8[...] = jnp.zeros_like(rec8)
     table[...] = jnp.zeros_like(table)
     ep_peers = [lax.rem(ep + d, n_ep) for d in far_first(n_ep)]
     tp_peers = [lax.rem(tp + d, n_tp) for d in far_first(n_tp)]
+    def ring_tp(r):
+        return jnp.where(2 * r < n_tp, 2 * r, 2 * (n_tp - 1 - r) + 1)
+
+    spot = jnp.where(lax.rem(tp, 2) == 0, tp // 2, n_tp - 1 - tp // 2)
+
     def tell(sem, reach):
         for d in (reach, n_tp - reach):
-            peer = lax.rem(tp + d, n_tp)
+            peer = ring_tp(lax.rem(spot + d, n_tp))
             pl.semaphore_signal(sem, inc=1, device_id={"tp": peer}, device_id_type=pl.DeviceIdType.MESH)
 
     tell(barrier, 1)
-
-    sources = (
-        tokens_h, gain1_h, wq_h, wk_h, wv_h, wo_h, win_h, wfg_h, ib_h, fb_h, hg_h, wp_h,
-        cell_h, norm_h, max_h, gain2_h, routes_h, rw_h, eg_h, eu_h, ed_h,
-    )
-    targets = (
-        tokens_v, gain1_v, wq_v, wk_v, wv_v, wo_v, win_v, wfg_v, ib_v, fb_v, hg_v, wp_v,
-        cell_v, norm_v, max_v, gain2_v, routes_v, rw_v, eg_v, eu_v, ed_v,
-    )
-    loads = [
-        pltpu.make_async_copy(s, t, load_sem.at[i]) for i, (s, t) in enumerate(zip(sources, targets))
-    ]
-    for copy in loads:
-        copy.start()
 
     place = lax.rem(ep + n_ep - 1, n_ep)
 
@@ -157,6 +161,8 @@
         lax.fori_loop(0, place, step, 0)
 
     to_those_below(statistics_to)
+    for copy in loads[6:]:
+        copy.start()
     for copy in loads[1:6]:
         copy.wait()
     gain_here = gain1_v[pl.ds(ep, 1), :]
@@ -451,12 +457,6 @@
     send(8, "tp", tp_peers, msg8, rec8, False, seq_local)
     rec8[tp] = layer16
     arrive(8, rec8, seq_local)
-    finished = jnp.concatenate([rec8[t].astype(F32) for t in range(n_tp)], axis=0).astype(BF16)
-    c8 = iota((seqs, SUB * n_tp), 1)
-    unpick = (c8 // SUB) * seq_local + c8 % SUB == iota((seqs, SUB * n_tp), 0)
-    unpick = unpick & (c8 % SUB < seq_local)
-    out_ref[...] = jnp.dot(unpick.astype(BF16), finished, preferred_element_type=F32).astype(BF16)
-
     @pl.when(place < n_ep - 2)
     def _():
         table_up.wait_send()
@@ -476,12 +476,22 @@
         settle(send_sem.at[phase], target, used_rows[phase - 1])
 
 
-def write_out(*refs):
-    *refs, sem = refs
-    count = len(refs) // 2
-    copies = [pltpu.make_async_copy(refs[i], refs[count + i], sem.at[i]) for i in range(count)]
-    for copy in copies:
+def write_out(seq_local, finished_ref, cell_ref, norm_ref, max_ref, out_h, cell_h, norm_h, max_h, out_v, sem):
+    copies = [
+        pltpu.make_async_copy(source, target, sem.at[i])
+        for i, (source, target) in enumerate(
+            ((cell_ref, cell_h), (norm_ref, norm_h), (max_ref, max_h), (out_v, out_h))
+        )
+    ]
+    for copy in copies[:3]:
         copy.start()
+    blocks, lanes = finished_ref.shape[0], finished_ref.shape[2]
+    finished = jnp.concatenate([finished_ref[t].astype(F32) for t in range(blocks)], axis=0).astype(BF16)
+    c8 = iota((out_v.shape[0], SUB * blocks), 1)
+    unpick = (c8 // SUB) * seq_local + c8 % SUB == iota(c8.shape, 0)
+    unpick = unpick & (c8 % SUB < seq_local)
+    out_v[...] = jnp.dot(unpick.astype(BF16), finished, preferred_element_type=F32).astype(BF16)
+    copies[3].start()
     for copy in copies:
         copy.wait()
 
@@ -530,11 +540,12 @@
             + pair((capacity * n_ep, LANES), (n_tp, capacity * n_ep, LANES), BF16)
             + pair((n_tp, capacity * n_ep, LANES), (n_tp, capacity * n_ep, LANES), BF16)
             + pair((n_ep, SUB, LANES), (n_ep, SUB, LANES), BF16)
-            + pair((SUB, LANES), (n_tp, SUB, LANES), BF16)
+            + [pltpu.VMEM((SUB, LANES), BF16)]
         )
         held = pl.pallas_call(
             functools.partial(kernel, n_ep, n_tp, seq_local, key_size, value_size),
-            out_shape=tuple(pltpu.VMEM(r.shape, r.dtype) for r in results),
+            out_shape=(pltpu.VMEM((n_tp, SUB, LANES), BF16),)
+            + tuple(pltpu.VMEM(r.shape, r.dtype) for r in results[1:]),
             in_specs=[hbm] * len(operands),
             out_specs=(vmem, vmem, vmem, vmem),
             scratch_shapes=[pltpu.VMEM(a.shape, a.dtype) for a in operands]
@@ -558,11 +569,11 @@
             ),
         )(*operands)
         out, new_cell, new_norm, new_max = pl.pallas_call(
-            write_out,
+            functools.partial(write_out, seq_local),
             out_shape=results,
-            in_specs=[pl.BlockSpec(memory_space=pl.ANY)] * len(results),
+            in_specs=[vmem] + [pl.BlockSpec(memory_space=pl.ANY)] * 3,
             out_specs=(hbm,) * len(results),
-            scratch_shapes=[pltpu.SemaphoreType.DMA((len(results),))],
+            scratch_shapes=[pltpu.VMEM(tokens.shape, BF16), pltpu.SemaphoreType.DMA((len(results),))],
             compiler_params=pltpu.CompilerParams(vmem_limit_bytes=1024 * 1024),
         )(*held)
         return out, new_cell, new_norm, new_max.T

time: 107 us -> 109 us (1.019)
    pallas_call x1, Pallas kernels: 106 us -> 107 us  [on_device(): pl.pallas_call(functools.partial(kernel, n_ep, n_tp, seq_local, key_size,...]
where the time goes in v5:
time: 109 us
  Pallas kernels  108 us (99%)
    pallas_call x1, Pallas kernels, on_device(): pl.pallas_call(functools.partial(kernel, n_ep, n_tp, seq_local, key_size,...  107 us

profile of v5, /device:TPU:65, one launch (start us, length us, event | category | flops | bytes accessed | tf_op | source)
XLA Modules:
  0.0 109.0 jit_solution(15828416019145743906)
XLA Ops:
  0.6 107.4 %shard_map.228 = (bf16[16,8,128]{2,1,0:T(8,128)(2,1)S(1)}, f32[6,1,128,256]{3,2,1,0:T(8,128)S(1)}, f32[6,1,128]{2,1,0:T(1,128)S(1)}, f32[1,6]{1,0:T(1,128)S(1)}) custom-call(bf16[96,128]{1,0:T(8,128)(2,1)} %tokens_h.1, f32[16,128]{1,0:T(8,128)} %bitcast.14, bf16[128,128]{1,0:T(8,128)(2,1)} %wq_h.1, bf16[128,128]{1,0:T(8,128)(2,1)} %wk_h.1, ...), custom_call_target="tpu_custom_call" | custom-call | tf_op jit(solution)/shard_map/pallas_call | solution.py:545
  108.0 0.9 shard_map.229

commit v6 on v5

--- a/solution.py
+++ b/solution.py
@@ -64,22 +64,18 @@
     table[...] = jnp.zeros_like(table)
     ep_peers = [lax.rem(ep + d, n_ep) for d in far_first(n_ep)]
     tp_peers = [lax.rem(tp + d, n_tp) for d in far_first(n_tp)]
-    def ring_tp(r):
-        return jnp.where(2 * r < n_tp, 2 * r, 2 * (n_tp - 1 - r) + 1)
-
-    spot = jnp.where(lax.rem(tp, 2) == 0, tp // 2, n_tp - 1 - tp // 2)
-
     def tell(sem, reach):
         for d in (reach, n_tp - reach):
-            peer = ring_tp(lax.rem(spot + d, n_tp))
+            peer = lax.rem(tp + d, n_tp)
             pl.semaphore_signal(sem, inc=1, device_id={"tp": peer}, device_id_type=pl.DeviceIdType.MESH)
 
     tell(barrier, 1)
 
-    place = lax.rem(ep + n_ep - 1, n_ep)
+    bottom = jnp.where(tp == 0, 1, 0)
+    place = lax.rem(ep + n_ep - bottom, n_ep)
 
     def at_place(q):
-        return lax.rem(q + 1, n_ep)
+        return lax.rem(q + bottom, n_ep)
 
     @pl.when(place == 0)
     def _():

time: 109 us -> 129 us (1.18)
  Pallas kernels: 108 us -> 128 us
    pallas_call x1, Pallas kernels: 107 us -> 127 us  [on_device(): pl.pallas_call(functools.partial(kernel, n_ep, n_tp, seq_local, key_size,...]
where the time goes in v6:
time: 129 us; the launch traced here: 128 us
  Pallas kernels  128 us (99%)
    pallas_call x1, Pallas kernels, on_device(): pl.pallas_call(functools.partial(kernel, n_ep, n_tp, seq_local, key_size,...  127 us

profile of v6, /device:TPU:65, one launch (start us, length us, event | category | flops | bytes accessed | tf_op | source)
XLA Modules:
  0.0 128.5 jit_solution(13478202094431007441)
XLA Ops:
  0.6 126.9 %shard_map.228 = (bf16[16,8,128]{2,1,0:T(8,128)(2,1)S(1)}, f32[6,1,128,256]{3,2,1,0:T(8,128)S(1)}, f32[6,1,128]{2,1,0:T(1,128)S(1)}, f32[1,6]{1,0:T(1,128)S(1)}) custom-call(bf16[96,128]{1,0:T(8,128)(2,1)} %tokens_h.1, f32[16,128]{1,0:T(8,128)} %bitcast.14, bf16[128,128]{1,0:T(8,128)(2,1)} %wq_h.1, bf16[128,128]{1,0:T(8,128)(2,1)} %wk_h.1, ...), custom_call_target="tpu_custom_call" | custom-call | tf_op jit(solution)/shard_map/pallas_call | solution.py:541
  127.5 0.9 shard_map.229
